TPU v7x, 32 devices: a whole 2x2x4 slice. The times are simulated.
32 devices in a mesh: fs: 4 (over y, x), tp: 8 (over z, core).
Axes of the slice: x: 2, y: 2, z: 4, core: 2. Of those that a mesh axis runs over, the one named last changes fastest.
Arguments:
- tokens: bfloat16 [4096, 2048], P(('fs', 'tp')), may hold values from -6 to 6
- gain: float32 [2048], P('fs'), may hold values from 0.1 to 1.9
- ex_gate: float32 [8, 256, 2048], P('tp', None, 'fs'), may hold values from -0.125 to 0.125
- ex_up: float32 [8, 256, 2048], P('tp', None, 'fs'), may hold values from -0.125 to 0.125
- ex_down: float32 [8, 256, 2048], P('tp', None, 'fs'), may hold values from -0.375 to 0.375
- sh_gate: float32 [512, 2048], P('tp', 'fs'), may hold values from -0.125 to 0.125
- sh_up: float32 [512, 2048], P('tp', 'fs'), may hold values from -0.125 to 0.125
- sh_down: float32 [512, 2048], P('tp', 'fs'), may hold values from -0.25 to 0.25
- routes: int32 [4096, 4], P(('fs', 'tp')), may hold values from 0 to 7, all different within a row; in each aligned block of 128 rows (0 to 127, 128 to 255, ...) at most 72 rows name the same one
- route_weight: float32 [4096, 4], P(('fs', 'tp')), may hold values from 0.1 to 1
Outputs:
- mixed: bfloat16 [4096, 2048], P(('fs', 'tp'))
- expert_gate: bfloat16 [8, 256, 2048], P('tp')
- expert_up: bfloat16 [8, 256, 2048], P('tp')
- expert_down: bfloat16 [8, 256, 2048], P('tp')
- shared_gate: bfloat16 [512, 2048], P('tp')
- shared_up: bfloat16 [512, 2048], P('tp')
- shared_down: bfloat16 [512, 2048], P('tp')
Inputs may be any that keep to these rules, and one draw needn't show every extreme that they name: `routes`: each row names 4 different experts. Among the rows of one device no expert is named by more than 72 rows, and in every draw some expert is named by exactly 72 rows of some device.
All inputs are finite; a program needn't handle non-finite values.
Results may differ from a plain program's by a relative error of at most 0.0085.
Values may be sent and summed in bfloat16 or wider, within the bound.
A program may use at most 64 MiB of HBM per device.

v0:
```python
import functools

import jax
import jax.numpy as jnp
from jax import lax
from jax.experimental import pallas as pl
from jax.experimental.pallas import tpu as pltpu
from jax.sharding import PartitionSpec as P

EPS = 1e-06
ROUTED_SCALE = 2.5
CONTRACT = (((1,), (1,)), ((), ()))
MESH = pl.DeviceIdType.MESH
LAG = 2
RING = 16
VMEM_LIMIT = 56 << 20


def kernel(
    F, T, H, S, M,
    tokens, gain, ex_gate, ex_up, ex_down, sh_gate, sh_up, sh_down, routes, rweight,
    wbuf, mix,
    tok, wt, hid_e, hid_s, own, pout, pin, sout, sin,
    ag_send, ag_recv, wt_send, wt_recv, w_send, w_recv,
    pout_sem, pin_sem, sout_sem, sin_sem,
    l_eg, l_eu, l_ed, l_sg, l_su, l_sd, load_sem,
):
    f = lax.axis_index("fs")
    me = lax.axis_index("tp")
    z = me // 2
    c = lax.rem(me, 2)
    Z = T // 2
    cw = wbuf.shape[2]
    rows = tokens.shape[0]
    GU = 2 * H + 2 * S
    ALL = 3 * H + 3 * S
    partner = 2 * z + 1 - c

    loads = [
        pltpu.make_async_copy(src, dst, load_sem.at[i])
        for i, (src, dst) in enumerate((
            (ex_gate, l_eg), (ex_up, l_eu), (sh_gate, l_sg), (sh_up, l_su), (ex_down, l_ed), (sh_down, l_sd)
        ))
    ]
    for load in loads:
        load.start()
    barrier = pltpu.get_barrier_semaphore()
    for i in range(1, F):
        pl.semaphore_signal(barrier, inc=1, device_id=(lax.rem(f + i, F), me), device_id_type=MESH)
    for i in range(1, T):
        pl.semaphore_signal(barrier, inc=1, device_id=(f, lax.rem(me + i, T)), device_id_type=MESH)

    values = tokens[...].astype(jnp.float32)
    inv = lax.rsqrt(jnp.mean(values * values, axis=1, keepdims=True) + EPS)
    tok[me] = (values * inv).astype(jnp.bfloat16)
    rw = rweight[...]
    w = rw / jnp.sum(rw, axis=0, keepdims=True) * ROUTED_SCALE
    ids = routes[...]
    expert = lax.broadcasted_iota(jnp.int32, (T, rows), 0)
    comb = jnp.zeros((T, rows), jnp.float32)
    for k in range(ids.shape[0]):
        comb = comb + jnp.where(expert == ids[k:k + 1, :], w[k:k + 1, :], 0.0)
    wt[me] = comb

    pl.semaphore_wait(barrier, F - 1 + T - 1)

    def rdma(src, dst, ssem, rsem, dev):
        return pltpu.make_async_remote_copy(
            src_ref=src, dst_ref=dst, send_sem=ssem, recv_sem=rsem,
            device_id=dev, device_id_type=MESH,
        )

    def tok_copy(s, way, t):
        return rdma(tok.at[s], tok.at[s], ag_send.at[s, way], ag_recv.at[s], (f, t))

    def w_copy(part, src, i, peer):
        lo, hi = ((0, GU), (GU, ALL))[part]
        return rdma(
            wbuf.at[src, lo:hi, :], wbuf.at[src, lo:hi, :],
            w_send.at[part, i], w_recv.at[part, src], (peer, me),
        )

    def wt_copy(s, i, t):
        return rdma(wt.at[s], wt.at[s], wt_send.at[i], wt_recv.at[s], (f, t))

    def right(t):
        return jnp.minimum(t + 2, T - 2 + lax.rem(t, 2))

    def left(t):
        return jnp.maximum(t - 2, lax.rem(t, 2))

    @pl.when(z < Z - 1)
    def _():
        tok_copy(me, 0, right(me)).start()

    @pl.when(z > 0)
    def _():
        tok_copy(me, 1, left(me)).start()

    tok_copy(me, 2, partner).start()
    for i in range(1, T):
        wt_copy(me, i, lax.rem(me + i, T)).start()
    for load in loads:
        load.wait()
    scale = gain[...]
    wbuf[f, 0:H, :] = (l_eg[...] * scale).astype(jnp.bfloat16)
    wbuf[f, H:2 * H, :] = (l_eu[...] * scale).astype(jnp.bfloat16)
    wbuf[f, 2 * H:2 * H + S, :] = (l_sg[...] * scale).astype(jnp.bfloat16)
    wbuf[f, 2 * H + S:GU, :] = (l_su[...] * scale).astype(jnp.bfloat16)
    wbuf[f, GU:GU + H, :] = l_ed[...].astype(jnp.bfloat16)
    wbuf[f, GU + H:ALL, :] = l_sd[...].astype(jnp.bfloat16)
    for i in range(1, F):
        w_copy(0, f, i, lax.rem(f + i, F)).start()
    for i in range(1, F):
        w_copy(1, f, i, lax.rem(f + i, F)).start()

    def gather_step(k, carry):
        a = me - 2 * k
        b = me + 2 * k

        @pl.when(a >= 0)
        def _():
            tok_copy(a, 0, partner).wait_recv()

            @pl.when(z < Z - 1)
            def _():
                tok_copy(a, 0, right(me)).start()

            tok_copy(a, 2, partner).start()

        @pl.when(b < T)
        def _():
            tok_copy(b, 1, partner).wait_recv()

            @pl.when(z > 0)
            def _():
                tok_copy(b, 1, left(me)).start()

            tok_copy(b, 2, partner).start()

        return carry

    lax.fori_loop(1, Z - 1, gather_step, 0)

    for i in range(1, F):
        w_copy(0, lax.rem(f + F - i, F), i, f).wait_recv()
    for i in range(1, T):
        wt_copy(lax.rem(me + T - i, T), i, me).wait_recv()

    def hidden_step(k, carry):
        tok_copy(2 * k + 1 - c, 0, partner).wait_recv()
        x = tok[pl.ds(2 * k, 2)].reshape(2 * rows, F * cw)
        acc = jnp.zeros((2 * rows, GU), jnp.float32)
        for q in range(F):
            acc = acc + lax.dot_general(
                x[:, q * cw:(q + 1) * cw], wbuf[q, 0:GU, :], CONTRACT,
                preferred_element_type=jnp.float32,
            )
        g, u = acc[:, 0:H], acc[:, H:2 * H]
        sg, su = acc[:, 2 * H:2 * H + S], acc[:, 2 * H + S:GU]
        he = g / (1.0 + jnp.exp(-g)) * u
        hs = sg / (1.0 + jnp.exp(-sg)) * su
        for h in range(2):
            row = wt[2 * k + h, pl.ds(me, 1), :]
            col = jnp.transpose(jnp.broadcast_to(row, (128, rows)))[:, 0:1]
            hid_e[2 * k + h] = (he[h * rows:(h + 1) * rows] * col).astype(jnp.bfloat16)
            hid_s[2 * k + h] = hs[h * rows:(h + 1) * rows].astype(jnp.bfloat16)
        return carry

    def near_step(k, carry):
        @pl.when(jnp.maximum(k - z, z - k) < Z - 1)
        def _():
            hidden_step(k, carry)

        return carry

    lax.fori_loop(0, Z, near_step, 0)
    gather_step(Z - 1, 0)

    @pl.when(z == 0)
    def _():
        hidden_step(Z - 1, 0)

    @pl.when(z == Z - 1)
    def _():
        hidden_step(0, 0)

    ring = pout.shape[0]
    big = Z * F
    near = jnp.minimum(jnp.where(z < Z - 1, z, big), jnp.where(z > 0, Z - 1 - z, big))
    count = Z * (F + Z - 1)

    def unit(n):
        s = n // Z
        i = lax.rem(n, Z)
        left_half = 2 * z < Z
        i = jnp.where(i == Z - 1, -1, i + jnp.where(i >= jnp.where(left_half, Z - 1 - z, z), 1, 0))
        d = jnp.where(i < 0, z, jnp.where(left_half, Z - 1 - i, i))
        away = jnp.where(d > z, z, jnp.where(d < z, Z - 1 - z, jnp.maximum(z, Z - 1 - z)))
        j = s - away
        return j, d, (j >= 0) & (j < F) & (n >= 0) & (n < count)

    def pair_copy(p, slot):
        return rdma(pout.at[p], pin.at[slot], pout_sem.at[p], pin_sem.at[slot], (f, partner))

    def sum_copy(p, slot, t):
        return rdma(sout.at[p], sin.at[slot], sout_sem.at[p], sin_sem.at[slot], (f, t))

    def produce(n, j, d, done):
        q = lax.rem(f + j, F)
        p = lax.rem(done, ring)
        he = hid_e[pl.ds(2 * d, 2)].reshape(2 * rows, H)
        hs = hid_s[pl.ds(2 * d, 2)].reshape(2 * rows, S)
        r = jnp.dot(he, wbuf[q, GU:GU + H, :], preferred_element_type=jnp.float32)
        r = r + jnp.dot(hs, wbuf[q, GU + H:ALL, :], preferred_element_type=jnp.float32)
        top, bottom = r[:rows], r[rows:]
        own[lax.rem(n, LAG + 1)] = jnp.where(c == 0, top, bottom)

        @pl.when(done >= ring)
        def _():
            pair_copy(p, 0).wait_send()

        pout[p] = jnp.where(c == 0, bottom, top).astype(jnp.bfloat16)
        pair_copy(p, j * Z + d).start()

    def finish(n, j, d, sent):
        q = lax.rem(f + j, F)
        o = lax.rem(n, LAG + 1)
        p = lax.rem(sent, ring)
        base = j * (Z + 1)
        pair_copy(0, j * Z + d).wait_recv()
        own[o] = own[o] + pin[j * Z + d].astype(jnp.float32)

        @pl.when((d >= z) & (z > 0))
        def _():
            sum_copy(0, base + d, me).wait_recv()
            own[o] = own[o] + sin[base + d].astype(jnp.float32)

        @pl.when((d <= z) & (z < Z - 1))
        def _():
            slot = base + jnp.where(d == z, Z, d)
            sum_copy(0, slot, me).wait_recv()
            own[o] = own[o] + sin[slot].astype(jnp.float32)

        @pl.when(d != z)
        def _():
            @pl.when(sent >= ring)
            def _():
                sum_copy(p, 0, partner).wait_send()

            sout[p] = own[o].astype(jnp.bfloat16)

            @pl.when(d > z)
            def _():
                sum_copy(p, base + d, right(me)).start()

            @pl.when(d < z)
            def _():
                sum_copy(p, base + jnp.where(d == z - 1, Z, d), left(me)).start()

        @pl.when(d == z)
        def _():
            mix[q] = own[o].astype(jnp.bfloat16)

    def sum_step(n, carry):
        done, sent = carry
        first = n // Z - near

        @pl.when((lax.rem(n, Z) == 0) & (first > 0) & (first < F))
        def _():
            w_copy(1, lax.rem(f + first, F), 1, f).wait_recv()

        j, d, valid = unit(n)

        @pl.when(valid)
        def _():
            produce(n, j, d, done)

        done = done + jnp.where(valid, 1, 0)
        m = n - LAG
        j, d, valid = unit(jnp.maximum(m, 0))
        valid = valid & (m >= 0)

        @pl.when(valid)
        def _():
            finish(m, j, d, sent)

        sent = sent + jnp.where(valid & (d != z), 1, 0)
        return done, sent

    lax.fori_loop(0, count + LAG, sum_step, (0, 0))

    for p in range(ring):
        pair_copy(p, 0).wait_send()
    for p in range(min(ring, (Z - 1) * F)):
        sum_copy(p, 0, partner).wait_send()
    for i in range(1, F):
        w_copy(0, f, i, lax.rem(f + i, F)).wait_send()
        w_copy(1, f, i, lax.rem(f + i, F)).wait_send()
    for i in range(1, T):
        wt_copy(me, i, lax.rem(me + i, T)).wait_send()

    def drain(k, carry):
        s = 2 * k + c

        @pl.when((k <= z) & (z < Z - 1))
        def _():
            tok_copy(s, 0, right(me)).wait_send()

        @pl.when((k >= z) & (z > 0))
        def _():
            tok_copy(s, 1, left(me)).wait_send()

        tok_copy(s, 2, partner).wait_send()
        return carry

    lax.fori_loop(0, Z, drain, 0)


def place(H, S, wbuf, mix, o_mixed, o_eg, o_eu, o_ed, o_sg, o_su, o_sd, sems):
    F, cw = wbuf.shape[0], wbuf.shape[2]
    GU = 2 * H + 2 * S
    pieces = ((o_eg, 0, H), (o_eu, H, H), (o_ed, GU, H), (o_sg, 2 * H, S), (o_su, 2 * H + S, S), (o_sd, GU + H, S))
    copies = []
    for p, (ref, lo, size) in enumerate(pieces):
        for q in range(F):
            copies.append(pltpu.make_async_copy(
                wbuf.at[q, lo:lo + size, :], ref.at[:, q * cw:(q + 1) * cw], sems.at[p, q]
            ))
    for q in range(F):
        copies.append(pltpu.make_async_copy(mix.at[q], o_mixed.at[:, q * cw:(q + 1) * cw], sems.at[6, q]))
    for copy in copies:
        copy.start()
    for copy in copies:
        copy.wait()


def local(F, T, tokens, gain, ex_gate, ex_up, ex_down, sh_gate, sh_up, sh_down, routes, route_weight):
    H, cw = ex_gate.shape[1:]
    S = sh_gate.shape[0]
    M = tokens.shape[0]
    D = tokens.shape[1]
    Z = T // 2
    N, U = (Z - 1) * F, Z * F
    ring = min(U, RING)
    bf, f32 = jnp.bfloat16, jnp.float32
    dma = pltpu.SemaphoreType.DMA
    wbuf, mix = pl.pallas_call(
        functools.partial(kernel, F, T, H, S, M),
        out_shape=[pltpu.VMEM((F, 3 * H + 3 * S, cw), bf), pltpu.VMEM((F, M, cw), bf)],
        in_specs=[pl.BlockSpec(memory_space=pltpu.VMEM)] * 2
        + [pl.BlockSpec(memory_space=pl.ANY)] * 6
        + [pl.BlockSpec(memory_space=pltpu.VMEM)] * 2,
        out_specs=[pl.BlockSpec(memory_space=pltpu.VMEM)] * 2,
        scratch_shapes=[
            pltpu.VMEM((T, M, D), bf),
            pltpu.VMEM((T, T, M), f32),
            pltpu.VMEM((T, M, H), bf),
            pltpu.VMEM((T, M, S), bf),
            pltpu.VMEM((LAG + 1, M, cw), f32),
            pltpu.VMEM((ring, M, cw), bf),
            pltpu.VMEM((U, M, cw), bf),
            pltpu.VMEM((ring, M, cw), bf),
            pltpu.VMEM((F * (Z + 1), M, cw), bf),
            dma((T, 3)),
            dma((T,)),
            dma((T,)),
            dma((T,)),
            dma((2, F)),
            dma((2, F)),
            dma((ring,)),
            dma((U,)),
            dma((ring,)),
            dma((F * (Z + 1),)),
            pltpu.VMEM((H, cw), f32),
            pltpu.VMEM((H, cw), f32),
            pltpu.VMEM((H, cw), f32),
            pltpu.VMEM((S, cw), f32),
            pltpu.VMEM((S, cw), f32),
            pltpu.VMEM((S, cw), f32),
            dma((6,)),
        ],
        compiler_params=pltpu.CompilerParams(
            collective_id=0, has_side_effects=True, vmem_limit_bytes=VMEM_LIMIT
        ),
    )(
        tokens, gain[None, :], ex_gate[0], ex_up[0], ex_down[0], sh_gate, sh_up, sh_down,
        routes.T, route_weight.T,
    )
    mixed, eg, eu, ed, sg, su, sd = pl.pallas_call(
        functools.partial(place, H, S),
        out_shape=[jax.ShapeDtypeStruct((M, D), bf)]
        + [jax.ShapeDtypeStruct((H, D), bf)] * 3
        + [jax.ShapeDtypeStruct((S, D), bf)] * 3,
        in_specs=[pl.BlockSpec(memory_space=pltpu.VMEM)] * 2,
        out_specs=[pl.BlockSpec(memory_space=pl.ANY)] * 7,
        scratch_shapes=[dma((7, F))],
        compiler_params=pltpu.CompilerParams(vmem_limit_bytes=4 << 20),
    )(pltpu.with_memory_space_constraint(wbuf, pltpu.VMEM), pltpu.with_memory_space_constraint(mix, pltpu.VMEM))
    return (mixed, eg[None], eu[None], ed[None], sg, su, sd)


def solution(mesh):
    in_specs = (
        P(("fs", "tp"), None),
        P("fs"),
        P("tp", None, "fs"),
        P("tp", None, "fs"),
        P("tp", None, "fs"),
        P("tp", "fs"),
        P("tp", "fs"),
        P("tp", "fs"),
        P(("fs", "tp"), None),
        P(("fs", "tp"), None),
    )
    out_specs = (
        P(("fs", "tp"), None),
        P("tp", None, None),
        P("tp", None, None),
        P("tp", None, None),
        P("tp", None),
        P("tp", None),
        P("tp", None),
    )
    step = functools.partial(local, mesh.shape["fs"], mesh.shape["tp"])
    return jax.shard_map(step, mesh=mesh, in_specs=in_specs, out_specs=out_specs, check_vma=False)
```

profile of v0, /device:TPU:0, one launch (start us, length us, event | category | flops | bytes accessed | tf_op | source)
XLA Modules:
  0.0 92.2 jit_solution(3725099365493831949)
XLA Ops:
  0.6 89.2 %shard_map.153 = (bf16[4,960,512]{2,1,0:T(8,128)(2,1)S(1)}, bf16[4,128,512]{2,1,0:T(8,128)(2,1)S(1)}) custom-call(bf16[128,2048]{1,0:T(8,128)(2,1)} %tokens.1, f32[1,512]{1,0:T(1,128)} %bitcast.12, f32[256,512]{1,0:T(8,128)} %bitcast.9, f32[256,512]{1,0:T(8,128)} %bitcast.10, f32[256,512]{1,0:T(8,128)} %bitcast.11, f32[64,512]{1,0:T(8,128)} %sh_gate.1, ...), custom_call_target="tpu_custom_call" | custom-call | tf_op jit(solution)/shard_map/pallas_call | solution.py:348
  89.9 2.3 %shard_map.154 = (bf16[128,2048]{1,0:T(8,128)(2,1)}, bf16[256,2048]{1,0:T(8,128)(2,1)}, bf16[256,2048]{1,0:T(8,128)(2,1)}, bf16[256,2048]{1,0:T(8,128)(2,1)}, bf...) custom-call(bf16[4,960,512]{2,1,0:T(8,128)(2,1)S(1)} %get-tuple-element.16.wbuf, ...), custom_call_target="tpu_custom_call" | custom-call | tf_op jit(solution)/shard_map/pallas_call | solution.py:390
where the time goes:
time: 92.3 us; the launch traced here: 92.2 us
  Pallas kernels  91.5 us (99%)
    pallas_call x1, Pallas kernels, local(): pl.pallas_call(functools.partial(kernel, F, T, H, S, M), out_shape=[pltpu...  89.2 us
    pallas_call x1, Pallas kernels, local(): pl.pallas_call(functools.partial(place, H, S), out_shape=[jax.ShapeDtypeS...  2.32 us

commit v1 on v0

--- a/solution.py
+++ b/solution.py
@@ -11,9 +11,13 @@
 ROUTED_SCALE = 2.5
 CONTRACT = (((1,), (1,)), ((), ()))
 MESH = pl.DeviceIdType.MESH
-LAG = 2
+PARTS = 2
 RING = 16
 VMEM_LIMIT = 56 << 20
+
+
+def halves(n):
+    return n // 32 * 16
 
 
 def kernel(
@@ -32,9 +36,15 @@
     Z = T // 2
     cw = wbuf.shape[2]
     rows = tokens.shape[0]
+    piece = rows // PARTS
     GU = 2 * H + 2 * S
     ALL = 3 * H + 3 * S
     partner = 2 * z + 1 - c
+    square = F == 4
+    fx = f + 1 - 2 * lax.rem(f, 2)
+    fy = lax.rem(f + 2, 4)
+    fd = 3 - f
+    late = Z >= 4
 
     loads = [
         pltpu.make_async_copy(src, dst, load_sem.at[i])
@@ -61,45 +71,6 @@
     for k in range(ids.shape[0]):
         comb = comb + jnp.where(expert == ids[k:k + 1, :], w[k:k + 1, :], 0.0)
     wt[me] = comb
-
-    pl.semaphore_wait(barrier, F - 1 + T - 1)
-
-    def rdma(src, dst, ssem, rsem, dev):
-        return pltpu.make_async_remote_copy(
-            src_ref=src, dst_ref=dst, send_sem=ssem, recv_sem=rsem,
-            device_id=dev, device_id_type=MESH,
-        )
-
-    def tok_copy(s, way, t):
-        return rdma(tok.at[s], tok.at[s], ag_send.at[s, way], ag_recv.at[s], (f, t))
-
-    def w_copy(part, src, i, peer):
-        lo, hi = ((0, GU), (GU, ALL))[part]
-        return rdma(
-            wbuf.at[src, lo:hi, :], wbuf.at[src, lo:hi, :],
-            w_send.at[part, i], w_recv.at[part, src], (peer, me),
-        )
-
-    def wt_copy(s, i, t):
-        return rdma(wt.at[s], wt.at[s], wt_send.at[i], wt_recv.at[s], (f, t))
-
-    def right(t):
-        return jnp.minimum(t + 2, T - 2 + lax.rem(t, 2))
-
-    def left(t):
-        return jnp.maximum(t - 2, lax.rem(t, 2))
-
-    @pl.when(z < Z - 1)
-    def _():
-        tok_copy(me, 0, right(me)).start()
-
-    @pl.when(z > 0)
-    def _():
-        tok_copy(me, 1, left(me)).start()
-
-    tok_copy(me, 2, partner).start()
-    for i in range(1, T):
-        wt_copy(me, i, lax.rem(me + i, T)).start()
     for load in loads:
         load.wait()
     scale = gain[...]
@@ -109,46 +80,122 @@
     wbuf[f, 2 * H + S:GU, :] = (l_su[...] * scale).astype(jnp.bfloat16)
     wbuf[f, GU:GU + H, :] = l_ed[...].astype(jnp.bfloat16)
     wbuf[f, GU + H:ALL, :] = l_sd[...].astype(jnp.bfloat16)
-    for i in range(1, F):
-        w_copy(0, f, i, lax.rem(f + i, F)).start()
-    for i in range(1, F):
-        w_copy(1, f, i, lax.rem(f + i, F)).start()
-
-    def gather_step(k, carry):
+
+    pl.semaphore_wait(barrier, F - 1 + T - 1)
+
+    def rdma(src, dst, ssem, rsem, dev):
+        return pltpu.make_async_remote_copy(
+            src_ref=src, dst_ref=dst, send_sem=ssem, recv_sem=rsem,
+            device_id=dev, device_id_type=MESH,
+        )
+
+    def tok_copy(s, h, way, t):
+        part = pl.ds(h * piece, piece)
+        return rdma(tok.at[s, part], tok.at[s, part], ag_send.at[s, h, way], ag_recv.at[s, h], (f, t))
+
+    if square:
+        bounds = (0, halves(GU), GU, GU + halves(ALL - GU), ALL)
+    else:
+        bounds = (0, GU, ALL)
+
+    def w_copy(part, src, i, peer):
+        lo, hi = bounds[part], bounds[part + 1]
+        return rdma(
+            wbuf.at[src, lo:hi, :], wbuf.at[src, lo:hi, :],
+            w_send.at[part, i], w_recv.at[part, src], (peer, me),
+        )
+
+    def wt_copy(s, i, t):
+        return rdma(wt.at[s], wt.at[s], wt_send.at[i], wt_recv.at[s], (f, t))
+
+    def right(t):
+        return jnp.minimum(t + 2, T - 2 + lax.rem(t, 2))
+
+    def left(t):
+        return jnp.maximum(t - 2, lax.rem(t, 2))
+
+    def own_weights(a, b):
+        w_copy(b, f, 0, fx).start()
+        w_copy(a, f, 1, fy).start()
+        w_copy(a, f, 0, fx).start()
+        w_copy(b, f, 1, fy).start()
+
+    def pass_weights(a, b):
+        w_copy(a, fy, 1, fy).wait_recv()
+        w_copy(a, fy, 2, fx).start()
+        w_copy(b, fx, 0, fx).wait_recv()
+        w_copy(b, fx, 2, fy).start()
+
+    for h in range(PARTS):
+        @pl.when(z < Z - 1)
+        def _():
+            tok_copy(me, h, 0, right(me)).start()
+
+        @pl.when(z > 0)
+        def _():
+            tok_copy(me, h, 1, left(me)).start()
+
+        tok_copy(me, h, 2, partner).start()
+
+    if square:
+        own_weights(0, 1)
+    else:
+        for part in range(2):
+            for i in range(1, F):
+                w_copy(part, f, i, lax.rem(f + i, F)).start()
+    for i in range(1, T):
+        wt_copy(me, i, lax.rem(me + i, T)).start()
+
+    def gather_piece(k, h):
         a = me - 2 * k
         b = me + 2 * k
 
         @pl.when(a >= 0)
         def _():
-            tok_copy(a, 0, partner).wait_recv()
+            tok_copy(a, h, 0, partner).wait_recv()
 
             @pl.when(z < Z - 1)
             def _():
-                tok_copy(a, 0, right(me)).start()
-
-            tok_copy(a, 2, partner).start()
+                tok_copy(a, h, 0, right(me)).start()
+
+            tok_copy(a, h, 2, partner).start()
 
         @pl.when(b < T)
         def _():
-            tok_copy(b, 1, partner).wait_recv()
+            tok_copy(b, h, 1, partner).wait_recv()
 
             @pl.when(z > 0)
             def _():
-                tok_copy(b, 1, left(me)).start()
-
-            tok_copy(b, 2, partner).start()
-
+                tok_copy(b, h, 1, left(me)).start()
+
+            tok_copy(b, h, 2, partner).start()
+
+    def gather_step(k, carry):
+        for h in range(PARTS):
+            gather_piece(k, h)
         return carry
 
-    lax.fori_loop(1, Z - 1, gather_step, 0)
-
-    for i in range(1, F):
-        w_copy(0, lax.rem(f + F - i, F), i, f).wait_recv()
+    for h in range(PARTS):
+        gather_piece(1, h)
+        if square and h == 0:
+            pass_weights(0, 1)
+            own_weights(2, 3)
+    lax.fori_loop(2, Z - 1 if late else Z, gather_step, 0)
+
+    if square:
+        w_copy(0, fx, 0, fx).wait_recv()
+        w_copy(1, fy, 1, fy).wait_recv()
+        w_copy(0, fd, 2, fx).wait_recv()
+        w_copy(1, fd, 2, fy).wait_recv()
+    else:
+        for i in range(1, F):
+            w_copy(0, lax.rem(f + F - i, F), i, f).wait_recv()
     for i in range(1, T):
         wt_copy(lax.rem(me + T - i, T), i, me).wait_recv()
 
     def hidden_step(k, carry):
-        tok_copy(2 * k + 1 - c, 0, partner).wait_recv()
+        for h in range(PARTS):
+            tok_copy(2 * k + 1 - c, h, 0, partner).wait_recv()
         x = tok[pl.ds(2 * k, 2)].reshape(2 * rows, F * cw)
         acc = jnp.zeros((2 * rows, GU), jnp.float32)
         for q in range(F):
@@ -167,38 +214,38 @@
             hid_s[2 * k + h] = hs[h * rows:(h + 1) * rows].astype(jnp.bfloat16)
         return carry
 
-    def near_step(k, carry):
-        @pl.when(jnp.maximum(k - z, z - k) < Z - 1)
+    def left_dest(k):
+        return jnp.where(k < Z - 2, Z - 3 - k, Z - 2)
+
+    end = (z == 0) | (z == Z - 1)
+    first = jnp.where(z == 0, Z - 1 - left_dest(0), left_dest(0))
+    last = Z - 1 - z
+
+    def early_step(k, carry):
+        @pl.when((k == first) | jnp.logical_not(end))
         def _():
             hidden_step(k, carry)
 
         return carry
 
-    lax.fori_loop(0, Z, near_step, 0)
-    gather_step(Z - 1, 0)
-
-    @pl.when(z == 0)
-    def _():
-        hidden_step(Z - 1, 0)
-
-    @pl.when(z == Z - 1)
-    def _():
-        hidden_step(0, 0)
+    def rest_step(k, carry):
+        @pl.when((k != first) & (k != last))
+        def _():
+            hidden_step(k, carry)
+
+        return carry
+
+    if late:
+        lax.fori_loop(0, Z, early_step, 0)
+    else:
+        lax.fori_loop(0, Z, hidden_step, 0)
 
     ring = pout.shape[0]
-    big = Z * F
-    near = jnp.minimum(jnp.where(z < Z - 1, z, big), jnp.where(z > 0, Z - 1 - z, big))
-    count = Z * (F + Z - 1)
-
-    def unit(n):
-        s = n // Z
-        i = lax.rem(n, Z)
-        left_half = 2 * z < Z
-        i = jnp.where(i == Z - 1, -1, i + jnp.where(i >= jnp.where(left_half, Z - 1 - z, z), 1, 0))
-        d = jnp.where(i < 0, z, jnp.where(left_half, Z - 1 - i, i))
-        away = jnp.where(d > z, z, jnp.where(d < z, Z - 1 - z, jnp.maximum(z, Z - 1 - z)))
-        j = s - away
-        return j, d, (j >= 0) & (j < F) & (n >= 0) & (n < count)
+
+    def chunk(j):
+        if square:
+            return jnp.where(j == 0, f, jnp.where(j == 1, fx, jnp.where(j == 2, fy, fd)))
+        return lax.rem(f + j, F)
 
     def pair_copy(p, slot):
         return rdma(pout.at[p], pin.at[slot], pout_sem.at[p], pin_sem.at[slot], (f, partner))
@@ -206,15 +253,15 @@
     def sum_copy(p, slot, t):
         return rdma(sout.at[p], sin.at[slot], sout_sem.at[p], sin_sem.at[slot], (f, t))
 
-    def produce(n, j, d, done):
-        q = lax.rem(f + j, F)
+    def produce(o, j, d, done):
+        q = chunk(j)
         p = lax.rem(done, ring)
         he = hid_e[pl.ds(2 * d, 2)].reshape(2 * rows, H)
         hs = hid_s[pl.ds(2 * d, 2)].reshape(2 * rows, S)
         r = jnp.dot(he, wbuf[q, GU:GU + H, :], preferred_element_type=jnp.float32)
         r = r + jnp.dot(hs, wbuf[q, GU + H:ALL, :], preferred_element_type=jnp.float32)
         top, bottom = r[:rows], r[rows:]
-        own[lax.rem(n, LAG + 1)] = jnp.where(c == 0, top, bottom)
+        own[o] = jnp.where(c == 0, top, bottom)
 
         @pl.when(done >= ring)
         def _():
@@ -223,9 +270,8 @@
         pout[p] = jnp.where(c == 0, bottom, top).astype(jnp.bfloat16)
         pair_copy(p, j * Z + d).start()
 
-    def finish(n, j, d, sent):
-        q = lax.rem(f + j, F)
-        o = lax.rem(n, LAG + 1)
+    def finish(o, j, d, sent):
+        q = chunk(j)
         p = lax.rem(sent, ring)
         base = j * (Z + 1)
         pair_copy(0, j * Z + d).wait_recv()
@@ -262,56 +308,100 @@
         def _():
             mix[q] = own[o].astype(jnp.bfloat16)
 
+    def side(k, s):
+        d = left_dest(jnp.minimum(k, Z - 2))
+        if s == 0:
+            d = jnp.where(k == Z - 1, z, d)
+            return d, (d < z) | (k == Z - 1)
+        d = Z - 1 - d
+        return d, (d > z) & (k < Z - 1)
+
+    def down_weights(j):
+        if square:
+            @pl.when(j == 1)
+            def _():
+                pass_weights(2, 3)
+                w_copy(2, fx, 0, fx).wait_recv()
+
+            @pl.when(j == 2)
+            def _():
+                w_copy(3, fy, 1, fy).wait_recv()
+
+            @pl.when(j == 3)
+            def _():
+                w_copy(2, fd, 2, fx).wait_recv()
+                w_copy(3, fd, 2, fy).wait_recv()
+        else:
+            @pl.when(j > 0)
+            def _():
+                w_copy(1, lax.rem(f + j, F), 1, f).wait_recv()
+
     def sum_step(n, carry):
         done, sent = carry
-        first = n // Z - near
-
-        @pl.when((lax.rem(n, Z) == 0) & (first > 0) & (first < F))
-        def _():
-            w_copy(1, lax.rem(f + first, F), 1, f).wait_recv()
-
-        j, d, valid = unit(n)
-
-        @pl.when(valid)
-        def _():
-            produce(n, j, d, done)
-
-        done = done + jnp.where(valid, 1, 0)
-        m = n - LAG
-        j, d, valid = unit(jnp.maximum(m, 0))
-        valid = valid & (m >= 0)
-
-        @pl.when(valid)
-        def _():
-            finish(m, j, d, sent)
-
-        sent = sent + jnp.where(valid & (d != z), 1, 0)
+        k = n // (F + 1)
+        j = lax.rem(n, F + 1)
+
+        if late:
+            @pl.when((n == F + 1) & end)
+            def _():
+                lax.fori_loop(0, Z, rest_step, 0)
+                gather_step(Z - 1, 0)
+                hidden_step(last, 0)
+
+        @pl.when((k == 0) & (j < F))
+        def _():
+            down_weights(j)
+
+        for s in range(2):
+            d, valid = side(k, s)
+            valid = valid & (j < F)
+
+            @pl.when(valid)
+            def _():
+                produce(2 * lax.rem(j, 2) + s, j, d, done)
+
+            done = done + jnp.where(valid, 1, 0)
+        for s in range(2):
+            d, valid = side(k, s)
+            valid = valid & (j > 0)
+
+            @pl.when(valid)
+            def _():
+                finish(2 * lax.rem(j + 1, 2) + s, j - 1, d, sent)
+
+            sent = sent + jnp.where(valid & (d != z), 1, 0)
         return done, sent
 
-    lax.fori_loop(0, count + LAG, sum_step, (0, 0))
+    lax.fori_loop(0, Z * (F + 1), sum_step, (0, 0))
 
     for p in range(ring):
         pair_copy(p, 0).wait_send()
     for p in range(min(ring, (Z - 1) * F)):
         sum_copy(p, 0, partner).wait_send()
-    for i in range(1, F):
-        w_copy(0, f, i, lax.rem(f + i, F)).wait_send()
-        w_copy(1, f, i, lax.rem(f + i, F)).wait_send()
+    if square:
+        for part in range(4):
+            w_copy(part, f, 0, fx).wait_send()
+            w_copy(part, f, 1, fy).wait_send()
+            w_copy(part, f, 2, fx).wait_send()
+    else:
+        for i in range(1, F):
+            w_copy(0, f, i, lax.rem(f + i, F)).wait_send()
+            w_copy(1, f, i, lax.rem(f + i, F)).wait_send()
     for i in range(1, T):
         wt_copy(me, i, lax.rem(me + i, T)).wait_send()
 
     def drain(k, carry):
         s = 2 * k + c
-
-        @pl.when((k <= z) & (z < Z - 1))
-        def _():
-            tok_copy(s, 0, right(me)).wait_send()
-
-        @pl.when((k >= z) & (z > 0))
-        def _():
-            tok_copy(s, 1, left(me)).wait_send()
-
-        tok_copy(s, 2, partner).wait_send()
+        for h in range(PARTS):
+            @pl.when((k <= z) & (z < Z - 1))
+            def _():
+                tok_copy(s, h, 0, right(me)).wait_send()
+
+            @pl.when((k >= z) & (z > 0))
+            def _():
+                tok_copy(s, h, 1, left(me)).wait_send()
+
+            tok_copy(s, h, 2, partner).wait_send()
         return carry
 
     lax.fori_loop(0, Z, drain, 0)
@@ -357,17 +447,17 @@
             pltpu.VMEM((T, T, M), f32),
             pltpu.VMEM((T, M, H), bf),
             pltpu.VMEM((T, M, S), bf),
-            pltpu.VMEM((LAG + 1, M, cw), f32),
+            pltpu.VMEM((4, M, cw), f32),
             pltpu.VMEM((ring, M, cw), bf),
             pltpu.VMEM((U, M, cw), bf),
             pltpu.VMEM((ring, M, cw), bf),
             pltpu.VMEM((F * (Z + 1), M, cw), bf),
-            dma((T, 3)),
+            dma((T, PARTS, 3)),
+            dma((T, PARTS)),
             dma((T,)),
             dma((T,)),
-            dma((T,)),
-            dma((2, F)),
-            dma((2, F)),
+            dma((4, F)),
+            dma((4, F)),
             dma((ring,)),
             dma((U,)),
             dma((ring,)),

time: 92.3 us -> 94.4 us (1.023)
  the two profiles are of different devices: /device:TPU:0 before, /device:TPU:17 now
where the time goes in v1:
time: 94.4 us; the launch traced here: 94.3 us
  Pallas kernels  93.6 us (99%)
    pallas_call x1, Pallas kernels, local(): pl.pallas_call(functools.partial(kernel, F, T, H, S, M), out_shape=[pltpu...  91.3 us
    pallas_call x1, Pallas kernels, local(): pl.pallas_call(functools.partial(place, H, S), out_shape=[jax.ShapeDtypeS...  2.32 us

profile of v1, /device:TPU:17, one launch (start us, length us, event | category | flops | bytes accessed | tf_op | source)
XLA Modules:
  0.0 94.3 jit_solution(16199416043384181391)
XLA Ops:
  0.6 91.3 %shard_map.153 = (bf16[4,960,512]{2,1,0:T(8,128)(2,1)S(1)}, bf16[4,128,512]{2,1,0:T(8,128)(2,1)S(1)}) custom-call(bf16[128,2048]{1,0:T(8,128)(2,1)} %tokens.1, f32[1,512]{1,0:T(1,128)} %bitcast.12, f32[256,512]{1,0:T(8,128)} %bitcast.9, f32[256,512]{1,0:T(8,128)} %bitcast.10, f32[256,512]{1,0:T(8,128)} %bitcast.11, f32[64,512]{1,0:T(8,128)} %sh_gate.1, ...), custom_call_target="tpu_custom_call" | custom-call | tf_op jit(solution)/shard_map/pallas_call | solution.py:438
  92.0 2.3 %shard_map.154 = (bf16[128,2048]{1,0:T(8,128)(2,1)}, bf16[256,2048]{1,0:T(8,128)(2,1)}, bf16[256,2048]{1,0:T(8,128)(2,1)}, bf16[256,2048]{1,0:T(8,128)(2,1)}, bf...) custom-call(bf16[4,960,512]{2,1,0:T(8,128)(2,1)S(1)} %get-tuple-element.16.wbuf, ...), custom_call_target="tpu_custom_call" | custom-call | tf_op jit(solution)/shard_map/pallas_call | solution.py:480

commit v2 on v1

--- a/solution.py
+++ b/solution.py
@@ -12,6 +12,8 @@
 CONTRACT = (((1,), (1,)), ((), ()))
 MESH = pl.DeviceIdType.MESH
 PARTS = 2
+AHEAD = 2
+SLOTS = AHEAD + 2
 RING = 16
 VMEM_LIMIT = 56 << 20
 
@@ -309,12 +311,10 @@
             mix[q] = own[o].astype(jnp.bfloat16)
 
     def side(k, s):
-        d = left_dest(jnp.minimum(k, Z - 2))
-        if s == 0:
-            d = jnp.where(k == Z - 1, z, d)
-            return d, (d < z) | (k == Z - 1)
-        d = Z - 1 - d
-        return d, (d > z) & (k < Z - 1)
+        d = left_dest(k)
+        to_left = jnp.where(2 * z < Z, s == 1, s == 0)
+        d = jnp.where(to_left, d, Z - 1 - d)
+        return d, jnp.where(to_left, d < z, d > z)
 
     def down_weights(j):
         if square:
@@ -336,13 +336,15 @@
             def _():
                 w_copy(1, lax.rem(f + j, F), 1, f).wait_recv()
 
+    steps = F + 1 + AHEAD
+
     def sum_step(n, carry):
         done, sent = carry
-        k = n // (F + 1)
-        j = lax.rem(n, F + 1)
+        k = n // steps
+        j = lax.rem(n, steps)
 
         if late:
-            @pl.when((n == F + 1) & end)
+            @pl.when((n == steps) & end)
             def _():
                 lax.fori_loop(0, Z, rest_step, 0)
                 gather_step(Z - 1, 0)
@@ -358,21 +360,33 @@
 
             @pl.when(valid)
             def _():
-                produce(2 * lax.rem(j, 2) + s, j, d, done)
+                produce(F + SLOTS * s + lax.rem(j, SLOTS), j, d, done)
 
             done = done + jnp.where(valid, 1, 0)
         for s in range(2):
             d, valid = side(k, s)
-            valid = valid & (j > 0)
+            i = j - 1 - AHEAD * s
+            valid = valid & (i >= 0) & (i < F)
 
             @pl.when(valid)
             def _():
-                finish(2 * lax.rem(j + 1, 2) + s, j - 1, d, sent)
-
-            sent = sent + jnp.where(valid & (d != z), 1, 0)
+                finish(F + SLOTS * s + lax.rem(jnp.maximum(i, 0), SLOTS), i, d, sent)
+
+            sent = sent + jnp.where(valid, 1, 0)
         return done, sent
 
-    lax.fori_loop(0, Z * (F + 1), sum_step, (0, 0))
+    done, sent = lax.fori_loop(0, (Z - 1) * steps, sum_step, (0, 0))
+
+    def own_produce(j, done):
+        produce(j, j, z, done)
+        return done + 1
+
+    def own_finish(j, carry):
+        finish(j, j, z, sent)
+        return carry
+
+    lax.fori_loop(0, F, own_produce, done)
+    lax.fori_loop(0, F, own_finish, 0)
 
     for p in range(ring):
         pair_copy(p, 0).wait_send()
@@ -447,7 +461,7 @@
             pltpu.VMEM((T, T, M), f32),
             pltpu.VMEM((T, M, H), bf),
             pltpu.VMEM((T, M, S), bf),
-            pltpu.VMEM((4, M, cw), f32),
+            pltpu.VMEM((F + 2 * SLOTS, M, cw), f32),
             pltpu.VMEM((ring, M, cw), bf),
             pltpu.VMEM((U, M, cw), bf),
             pltpu.VMEM((ring, M, cw), bf),

time: 94.4 us -> 77 us (0.82)
  the two profiles are of different devices: /device:TPU:17 before, /device:TPU:0 now
where the time goes in v2:
time: 77 us; the launch traced here: 76.8 us
  Pallas kernels  76.2 us (99%)
    pallas_call x1, Pallas kernels, local(): pl.pallas_call(functools.partial(kernel, F, T, H, S, M), out_shape=[pltpu...  73.9 us
    pallas_call x1, Pallas kernels, local(): pl.pallas_call(functools.partial(place, H, S), out_shape=[jax.ShapeDtypeS...  2.32 us

profile of v2, /device:TPU:0, one launch (start us, length us, event | category | flops | bytes accessed | tf_op | source)
XLA Modules:
  0.0 76.8 jit_solution(6839350643851122972)
XLA Ops:
  0.6 73.9 %shard_map.153 = (bf16[4,960,512]{2,1,0:T(8,128)(2,1)S(1)}, bf16[4,128,512]{2,1,0:T(8,128)(2,1)S(1)}) custom-call(bf16[128,2048]{1,0:T(8,128)(2,1)} %tokens.1, f32[1,512]{1,0:T(1,128)} %bitcast.12, f32[256,512]{1,0:T(8,128)} %bitcast.9, f32[256,512]{1,0:T(8,128)} %bitcast.10, f32[256,512]{1,0:T(8,128)} %bitcast.11, f32[64,512]{1,0:T(8,128)} %sh_gate.1, ...), custom_call_target="tpu_custom_call" | custom-call | tf_op jit(solution)/shard_map/pallas_call | solution.py:452
  74.5 2.3 %shard_map.154 = (bf16[128,2048]{1,0:T(8,128)(2,1)}, bf16[256,2048]{1,0:T(8,128)(2,1)}, bf16[256,2048]{1,0:T(8,128)(2,1)}, bf16[256,2048]{1,0:T(8,128)(2,1)}, bf...) custom-call(bf16[4,960,512]{2,1,0:T(8,128)(2,1)S(1)} %get-tuple-element.16.wbuf, ...), custom_call_target="tpu_custom_call" | custom-call | tf_op jit(solution)/shard_map/pallas_call | solution.py:494

commit v3 on v2

--- a/solution.py
+++ b/solution.py
@@ -11,8 +11,10 @@
 ROUTED_SCALE = 2.5
 CONTRACT = (((1,), (1,)), ((), ()))
 MESH = pl.DeviceIdType.MESH
-PARTS = 2
-AHEAD = 2
+PARTS = 4
+HELD = 2
+SPLIT = 4
+AHEAD = 1
 SLOTS = AHEAD + 2
 RING = 16
 VMEM_LIMIT = 56 << 20
@@ -26,10 +28,10 @@
     F, T, H, S, M,
     tokens, gain, ex_gate, ex_up, ex_down, sh_gate, sh_up, sh_down, routes, rweight,
     wbuf, mix,
-    tok, wt, hid_e, hid_s, own, pout, pin, sout, sin,
-    ag_send, ag_recv, wt_send, wt_recv, w_send, w_recv,
-    pout_sem, pin_sem, sout_sem, sin_sem,
-    l_eg, l_eu, l_ed, l_sg, l_su, l_sd, load_sem,
+    tok, wt, hid, own, pout, pin, sout, sin, down2, hid2,
+    ag_send, ag_recv, pair_sent, wt_send, wt_recv, w_send, w_recv,
+    pout_sem, pin_sem, sout_sem, sin_sem, d2_send, d2_recv, z_send, z_recv,
+    l_eg, l_eu, l_ed, l_sg, l_su, l_sd, l_tok, l_gain, l_ids, l_rw, load_sem,
 ):
     f = lax.axis_index("fs")
     me = lax.axis_index("tp")
@@ -37,7 +39,7 @@
     c = lax.rem(me, 2)
     Z = T // 2
     cw = wbuf.shape[2]
-    rows = tokens.shape[0]
+    rows = M
     piece = rows // PARTS
     GU = 2 * H + 2 * S
     ALL = 3 * H + 3 * S
@@ -47,35 +49,42 @@
     fy = lax.rem(f + 2, 4)
     fd = 3 - f
     late = Z >= 4
-
-    loads = [
-        pltpu.make_async_copy(src, dst, load_sem.at[i])
-        for i, (src, dst) in enumerate((
-            (ex_gate, l_eg), (ex_up, l_eu), (sh_gate, l_sg), (sh_up, l_su), (ex_down, l_ed), (sh_down, l_sd)
-        ))
-    ]
-    for load in loads:
-        load.start()
+    HS = H + S
+    strip = rows // SPLIT
+    end = (z == 0) | (z == Z - 1)
+    near = (z == 1) | (z == Z - 2)
+
     barrier = pltpu.get_barrier_semaphore()
     for i in range(1, F):
         pl.semaphore_signal(barrier, inc=1, device_id=(lax.rem(f + i, F), me), device_id_type=MESH)
     for i in range(1, T):
         pl.semaphore_signal(barrier, inc=1, device_id=(f, lax.rem(me + i, T)), device_id_type=MESH)
-
-    values = tokens[...].astype(jnp.float32)
+    loads = [
+        pltpu.make_async_copy(src, dst, load_sem.at[i])
+        for i, (src, dst) in enumerate((
+            (tokens, l_tok), (routes, l_ids), (rweight, l_rw), (gain, l_gain),
+            (ex_gate, l_eg), (ex_up, l_eu), (sh_gate, l_sg), (sh_up, l_su), (ex_down, l_ed), (sh_down, l_sd),
+        ))
+    ]
+    for load in loads:
+        load.start()
+
+    for load in loads[:4]:
+        load.wait()
+    values = l_tok[...].astype(jnp.float32)
     inv = lax.rsqrt(jnp.mean(values * values, axis=1, keepdims=True) + EPS)
     tok[me] = (values * inv).astype(jnp.bfloat16)
-    rw = rweight[...]
+    rw = l_rw[...]
     w = rw / jnp.sum(rw, axis=0, keepdims=True) * ROUTED_SCALE
-    ids = routes[...]
+    ids = l_ids[...]
     expert = lax.broadcasted_iota(jnp.int32, (T, rows), 0)
     comb = jnp.zeros((T, rows), jnp.float32)
     for k in range(ids.shape[0]):
         comb = comb + jnp.where(expert == ids[k:k + 1, :], w[k:k + 1, :], 0.0)
     wt[me] = comb
-    for load in loads:
+    for load in loads[4:]:
         load.wait()
-    scale = gain[...]
+    scale = l_gain[...]
     wbuf[f, 0:H, :] = (l_eg[...] * scale).astype(jnp.bfloat16)
     wbuf[f, H:2 * H, :] = (l_eu[...] * scale).astype(jnp.bfloat16)
     wbuf[f, 2 * H:2 * H + S, :] = (l_sg[...] * scale).astype(jnp.bfloat16)
@@ -93,7 +102,8 @@
 
     def tok_copy(s, h, way, t):
         part = pl.ds(h * piece, piece)
-        return rdma(tok.at[s, part], tok.at[s, part], ag_send.at[s, h, way], ag_recv.at[s, h], (f, t))
+        sem = ag_send.at[s, way] if way < 2 else pair_sent.at[0]
+        return rdma(tok.at[s, part], tok.at[s, part], sem, ag_recv.at[s, h], (f, t))
 
     if square:
         bounds = (0, halves(GU), GU, GU + halves(ALL - GU), ALL)
@@ -104,11 +114,15 @@
         lo, hi = bounds[part], bounds[part + 1]
         return rdma(
             wbuf.at[src, lo:hi, :], wbuf.at[src, lo:hi, :],
-            w_send.at[part, i], w_recv.at[part, src], (peer, me),
+            w_send.at[0 if square else part, i], w_recv.at[part, src], (peer, me),
         )
 
     def wt_copy(s, i, t):
-        return rdma(wt.at[s], wt.at[s], wt_send.at[i], wt_recv.at[s], (f, t))
+        return rdma(wt.at[s], wt.at[s], wt_send.at[0], wt_recv.at[0], (f, t))
+
+    def wt_all():
+        block = wt.at[pl.ds(0, T - 1)]
+        return rdma(block, block, wt_send.at[0], wt_recv.at[0], (f, partner))
 
     def right(t):
         return jnp.minimum(t + 2, T - 2 + lax.rem(t, 2))
@@ -128,16 +142,40 @@
         w_copy(b, fx, 0, fx).wait_recv()
         w_copy(b, fx, 2, fy).start()
 
+    hold_right = (z == Z - 2) if late else (z < 0)
+    hold_left = (z == 1) if late else (z < 0)
     for h in range(PARTS):
-        @pl.when(z < Z - 1)
+        go_right, go_left = z < Z - 1, z > 0
+        if h >= PARTS - HELD:
+            go_right = go_right & jnp.logical_not(hold_right)
+            go_left = go_left & jnp.logical_not(hold_left)
+
+        @pl.when(go_right)
         def _():
             tok_copy(me, h, 0, right(me)).start()
 
-        @pl.when(z > 0)
+        @pl.when(go_left)
         def _():
             tok_copy(me, h, 1, left(me)).start()
 
         tok_copy(me, h, 2, partner).start()
+
+    inner = jnp.where(z == 0, me + 2, jnp.where(z == Z - 1, me - 2, partner))
+
+    def end_weights():
+        return rdma(wbuf.at[f, GU:ALL, :], down2.at[f], z_send.at[0], z_recv.at[0], (f, inner))
+
+    def end_hidden(h):
+        part = pl.ds(h * (rows // 2), rows // 2)
+        return rdma(
+            hid.at[pl.ds(2 * (inner // 2), 2), part], hid2.at[:, part],
+            z_send.at[1 + h], z_recv.at[1 + h], (f, inner),
+        )
+
+    if late:
+        @pl.when(end)
+        def _():
+            end_weights().start()
 
     if square:
         own_weights(0, 1)
@@ -178,11 +216,26 @@
         return carry
 
     for h in range(PARTS):
-        gather_piece(1, h)
-        if square and h == 0:
+        if late and h >= PARTS - HELD:
+            @pl.when(jnp.logical_not(end))
+            def _():
+                gather_piece(1, h)
+        else:
+            gather_piece(1, h)
+        if square and h == 1:
             pass_weights(0, 1)
             own_weights(2, 3)
     lax.fori_loop(2, Z - 1 if late else Z, gather_step, 0)
+    if late:
+        for h in range(PARTS - HELD, PARTS):
+            @pl.when(hold_right)
+            def _():
+                tok_copy(me, h, 0, right(me)).start()
+
+            @pl.when(hold_left)
+            def _():
+                tok_copy(me, h, 1, left(me)).start()
+
 
     if square:
         w_copy(0, fx, 0, fx).wait_recv()
@@ -192,14 +245,14 @@
     else:
         for i in range(1, F):
             w_copy(0, lax.rem(f + F - i, F), i, f).wait_recv()
-    for i in range(1, T):
-        wt_copy(lax.rem(me + T - i, T), i, me).wait_recv()
-
-    def hidden_step(k, carry):
-        for h in range(PARTS):
+    wt_all().wait_recv()
+
+    def hidden_rows(k, parts):
+        lo, n = parts[0] * piece, len(parts) * piece
+        for h in parts:
             tok_copy(2 * k + 1 - c, h, 0, partner).wait_recv()
-        x = tok[pl.ds(2 * k, 2)].reshape(2 * rows, F * cw)
-        acc = jnp.zeros((2 * rows, GU), jnp.float32)
+        x = tok[pl.ds(2 * k, 2), lo:lo + n].reshape(2 * n, F * cw)
+        acc = jnp.zeros((2 * n, GU), jnp.float32)
         for q in range(F):
             acc = acc + lax.dot_general(
                 x[:, q * cw:(q + 1) * cw], wbuf[q, 0:GU, :], CONTRACT,
@@ -211,15 +264,19 @@
         hs = sg / (1.0 + jnp.exp(-sg)) * su
         for h in range(2):
             row = wt[2 * k + h, pl.ds(me, 1), :]
-            col = jnp.transpose(jnp.broadcast_to(row, (128, rows)))[:, 0:1]
-            hid_e[2 * k + h] = (he[h * rows:(h + 1) * rows] * col).astype(jnp.bfloat16)
-            hid_s[2 * k + h] = hs[h * rows:(h + 1) * rows].astype(jnp.bfloat16)
+            col = jnp.transpose(jnp.broadcast_to(row, (128, rows)))[lo:lo + n, 0:1]
+            hid[2 * k + h, lo:lo + n, 0:H] = (he[h * n:(h + 1) * n] * col).astype(jnp.bfloat16)
+            hid[2 * k + h, lo:lo + n, H:HS] = hs[h * n:(h + 1) * n].astype(jnp.bfloat16)
+            if hid.shape[2] > HS:
+                hid[2 * k + h, lo:lo + n, HS:] = jnp.zeros((n, hid.shape[2] - HS), jnp.bfloat16)
+
+    def hidden_step(k, carry):
+        hidden_rows(k, range(PARTS))
         return carry
 
     def left_dest(k):
         return jnp.where(k < Z - 2, Z - 3 - k, Z - 2)
 
-    end = (z == 0) | (z == Z - 1)
     first = jnp.where(z == 0, Z - 1 - left_dest(0), left_dest(0))
     last = Z - 1 - z
 
@@ -231,7 +288,7 @@
         return carry
 
     def rest_step(k, carry):
-        @pl.when((k != first) & (k != last))
+        @pl.when((k != first) & (k != last) & (k != inner // 2))
         def _():
             hidden_step(k, carry)
 
@@ -243,6 +300,7 @@
         lax.fori_loop(0, Z, hidden_step, 0)
 
     ring = pout.shape[0]
+    reuse = Z * F > ring
 
     def chunk(j):
         if square:
@@ -250,26 +308,39 @@
         return lax.rem(f + j, F)
 
     def pair_copy(p, slot):
-        return rdma(pout.at[p], pin.at[slot], pout_sem.at[p], pin_sem.at[slot], (f, partner))
-
-    def sum_copy(p, slot, t):
-        return rdma(sout.at[p], sin.at[slot], sout_sem.at[p], sin_sem.at[slot], (f, t))
-
-    def produce(o, j, d, done):
+        return rdma(pout.at[p], pin.at[slot], pout_sem.at[p if reuse else 0], pin_sem.at[slot], (f, partner))
+
+    def sum_copy(p, h, slot, t):
+        part = pl.ds(h * strip, strip)
+        return rdma(sout.at[p, part], sin.at[slot, part], sout_sem.at[p, h] if reuse else sout_sem.at[0, 0], sin_sem.at[slot, h], (f, t))
+
+    def share(o, r, p):
+        top, bottom = r[:rows], r[rows:]
+        own[o] = jnp.where(c == 0, top, bottom)
+        pout[p] = jnp.where(c == 0, bottom, top).astype(jnp.bfloat16)
+
+    def produce(o, j, d, done, extra=False):
         q = chunk(j)
         p = lax.rem(done, ring)
-        he = hid_e[pl.ds(2 * d, 2)].reshape(2 * rows, H)
-        hs = hid_s[pl.ds(2 * d, 2)].reshape(2 * rows, S)
-        r = jnp.dot(he, wbuf[q, GU:GU + H, :], preferred_element_type=jnp.float32)
-        r = r + jnp.dot(hs, wbuf[q, GU + H:ALL, :], preferred_element_type=jnp.float32)
-        top, bottom = r[:rows], r[rows:]
-        own[o] = jnp.where(c == 0, top, bottom)
-
-        @pl.when(done >= ring)
-        def _():
-            pair_copy(p, 0).wait_send()
-
-        pout[p] = jnp.where(c == 0, bottom, top).astype(jnp.bfloat16)
+        x = hid[pl.ds(2 * d, 2)].reshape(2 * rows, hid.shape[2])[:, 0:HS]
+        r = jnp.dot(x, wbuf[q, GU:ALL, :], preferred_element_type=jnp.float32)
+
+        if reuse:
+            @pl.when(done >= ring)
+            def _():
+                pair_copy(p, 0).wait_send()
+
+        if extra:
+            @pl.when(near)
+            def _():
+                y = hid2[...].reshape(2 * rows, hid.shape[2])[:, 0:HS]
+                share(o, r + jnp.dot(y, down2[q], preferred_element_type=jnp.float32), p)
+
+            @pl.when(jnp.logical_not(near))
+            def _():
+                share(o, r, p)
+        else:
+            share(o, r, p)
         pair_copy(p, j * Z + d).start()
 
     def finish(o, j, d, sent):
@@ -278,33 +349,44 @@
         base = j * (Z + 1)
         pair_copy(0, j * Z + d).wait_recv()
         own[o] = own[o] + pin[j * Z + d].astype(jnp.float32)
-
-        @pl.when((d >= z) & (z > 0))
-        def _():
-            sum_copy(0, base + d, me).wait_recv()
-            own[o] = own[o] + sin[base + d].astype(jnp.float32)
-
-        @pl.when((d <= z) & (z < Z - 1))
-        def _():
-            slot = base + jnp.where(d == z, Z, d)
-            sum_copy(0, slot, me).wait_recv()
-            own[o] = own[o] + sin[slot].astype(jnp.float32)
-
-        @pl.when(d != z)
-        def _():
-            @pl.when(sent >= ring)
-            def _():
-                sum_copy(p, 0, partner).wait_send()
-
-            sout[p] = own[o].astype(jnp.bfloat16)
+        if late:
+            from_left = (z > 0) & ((d > z) | ((d == z) & (z > 1)))
+            from_right = (z < Z - 1) & ((d < z) | ((d == z) & (z < Z - 2)))
+        else:
+            from_left = (d >= z) & (z > 0)
+            from_right = (d <= z) & (z < Z - 1)
+
+        if reuse:
+            @pl.when((d != z) & (sent >= ring))
+            def _():
+                for h in range(SPLIT):
+                    sum_copy(p, h, 0, partner).wait_send()
+
+        for h in range(SPLIT):
+            part = pl.ds(h * strip, strip)
+
+            @pl.when(from_left)
+            def _():
+                sum_copy(0, h, base + d, me).wait_recv()
+                own[o, part] = own[o, part] + sin[base + d, part].astype(jnp.float32)
+
+            @pl.when(from_right)
+            def _():
+                slot = base + jnp.where(d == z, Z, d)
+                sum_copy(0, h, slot, me).wait_recv()
+                own[o, part] = own[o, part] + sin[slot, part].astype(jnp.float32)
+
+            @pl.when(d != z)
+            def _():
+                sout[p, part] = own[o, part].astype(jnp.bfloat16)
 
             @pl.when(d > z)
             def _():
-                sum_copy(p, base + d, right(me)).start()
+                sum_copy(p, h, base + d, right(me)).start()
 
             @pl.when(d < z)
             def _():
-                sum_copy(p, base + jnp.where(d == z - 1, Z, d), left(me)).start()
+                sum_copy(p, h, base + jnp.where(d == z - 1, Z, d), left(me)).start()
 
         @pl.when(d == z)
         def _():
@@ -337,6 +419,49 @@
                 w_copy(1, lax.rem(f + j, F), 1, f).wait_recv()
 
     steps = F + 1 + AHEAD
+    if square:
+        bounds2 = (0, halves(HS), HS)
+    else:
+        bounds2 = (0, HS)
+
+    def d2_copy(part, src, i, peer):
+        lo, hi = bounds2[part], bounds2[part + 1]
+        return rdma(
+            down2.at[src, lo:hi, :], down2.at[src, lo:hi, :],
+            d2_send.at[0, i], d2_recv.at[part, src], (peer, me),
+        )
+
+    def d2_own():
+        end_weights().wait_recv()
+        if square:
+            d2_copy(1, f, 0, fx).start()
+            d2_copy(0, f, 1, fy).start()
+            d2_copy(0, f, 0, fx).start()
+            d2_copy(1, f, 1, fy).start()
+        else:
+            for i in range(1, F):
+                d2_copy(0, f, i, lax.rem(f + i, F)).start()
+
+    def d2_pass():
+        if square:
+            d2_copy(0, fy, 1, fy).wait_recv()
+            d2_copy(0, fy, 2, fx).start()
+            d2_copy(1, fx, 0, fx).wait_recv()
+            d2_copy(1, fx, 2, fy).start()
+
+    def d2_rest():
+        if square:
+            d2_copy(0, fx, 0, fx).wait_recv()
+            d2_copy(1, fy, 1, fy).wait_recv()
+            d2_copy(0, fd, 2, fx).wait_recv()
+            d2_copy(1, fd, 2, fy).wait_recv()
+        else:
+            for i in range(1, F):
+                d2_copy(0, lax.rem(f + F - i, F), i, f).wait_recv()
+
+    def d2_sent():
+        for i in range(3) if square else range(1, F):
+            rdma(down2.at[f], down2.at[f], d2_send.at[0, i], d2_recv.at[0, f], (fx if square else f, me)).wait_send()
 
     def sum_step(n, carry):
         done, sent = carry
@@ -346,13 +471,38 @@
         if late:
             @pl.when((n == steps) & end)
             def _():
-                lax.fori_loop(0, Z, rest_step, 0)
                 gather_step(Z - 1, 0)
+                if Z > 4:
+                    lax.fori_loop(0, Z, rest_step, 0)
                 hidden_step(last, 0)
 
+            @pl.when((n == steps) & near)
+            def _():
+                d2_pass()
+
+        if late:
+            d, valid = side(k, 0)
+            valid = valid & end & (k == 0) & (j > 0) & (j <= F)
+
+            @pl.when(valid)
+            def _():
+                finish(F + lax.rem(j + SLOTS - 1, SLOTS), j - 1, d, sent)
+
+            sent = sent + jnp.where(valid, 1, 0)
+
+            @pl.when((n == 1) & end)
+            def _():
+                hidden_rows(inner // 2, range(PARTS - HELD))
+                end_hidden(0).start()
+
         @pl.when((k == 0) & (j < F))
         def _():
             down_weights(j)
+
+        if late:
+            @pl.when((n == 2) & near)
+            def _():
+                d2_own()
 
         for s in range(2):
             d, valid = side(k, s)
@@ -367,6 +517,8 @@
             d, valid = side(k, s)
             i = j - 1 - AHEAD * s
             valid = valid & (i >= 0) & (i < F)
+            if late and s == 0:
+                valid = valid & jnp.logical_not(end & (k == 0))
 
             @pl.when(valid)
             def _():
@@ -375,50 +527,110 @@
             sent = sent + jnp.where(valid, 1, 0)
         return done, sent
 
-    done, sent = lax.fori_loop(0, (Z - 1) * steps, sum_step, (0, 0))
+    done, sent = lax.fori_loop(0, (Z - 2 if late else Z - 1) * steps, sum_step, (0, 0))
+    if late:
+        @pl.when(end)
+        def _():
+            for h in range(PARTS - HELD, PARTS):
+                gather_piece(1, h)
+            hidden_rows(inner // 2, range(PARTS - HELD, PARTS))
+            end_hidden(1).start()
+            if Z == 4:
+                hidden_step(z, 0)
+
+        @pl.when(near)
+        def _():
+            d2_rest()
+            for h in range(2):
+                end_hidden(h).wait_recv()
 
     def own_produce(j, done):
-        produce(j, j, z, done)
+        produce(j, j, z, done, late)
         return done + 1
 
     def own_finish(j, carry):
         finish(j, j, z, sent)
         return carry
 
-    lax.fori_loop(0, F, own_produce, done)
-    lax.fori_loop(0, F, own_finish, 0)
-
-    for p in range(ring):
-        pair_copy(p, 0).wait_send()
-    for p in range(min(ring, (Z - 1) * F)):
-        sum_copy(p, 0, partner).wait_send()
+    done = lax.fori_loop(0, F, own_produce, done)
+    def pair_all(n):
+        src, dst = pout.at[pl.ds(0, n)], pin.at[pl.ds(0, n)]
+        return rdma(src, dst, pout_sem.at[0], pin_sem.at[0], (f, partner))
+
+    def sum_all(n):
+        src, dst = sout.at[pl.ds(0, n)], sin.at[pl.ds(0, n)]
+        return rdma(src, dst, sout_sem.at[0, 0], sin_sem.at[0, 0], (f, partner))
+
     if square:
-        for part in range(4):
-            w_copy(part, f, 0, fx).wait_send()
-            w_copy(part, f, 1, fy).wait_send()
-            w_copy(part, f, 2, fx).wait_send()
+        for i in range(3):
+            rdma(wbuf.at[f], wbuf.at[f], w_send.at[0, i], w_recv.at[0, f], (fx, me)).wait_send()
     else:
         for i in range(1, F):
             w_copy(0, f, i, lax.rem(f + i, F)).wait_send()
             w_copy(1, f, i, lax.rem(f + i, F)).wait_send()
-    for i in range(1, T):
-        wt_copy(me, i, lax.rem(me + i, T)).wait_send()
+    wt_all().wait_send()
+
+    def block_sent(s, way, t):
+        return rdma(tok.at[s], tok.at[s], ag_send.at[s, way], ag_recv.at[s, 0], (f, t))
 
     def drain(k, carry):
         s = 2 * k + c
-        for h in range(PARTS):
-            @pl.when((k <= z) & (z < Z - 1))
-            def _():
-                tok_copy(s, h, 0, right(me)).wait_send()
-
-            @pl.when((k >= z) & (z > 0))
-            def _():
-                tok_copy(s, h, 1, left(me)).wait_send()
-
-            tok_copy(s, h, 2, partner).wait_send()
+
+        @pl.when((k <= z) & (z < Z - 1))
+        def _():
+            block_sent(s, 0, right(me)).wait_send()
+
+        @pl.when((k >= z) & (z > 0))
+        def _():
+            block_sent(s, 1, left(me)).wait_send()
+
         return carry
 
     lax.fori_loop(0, Z, drain, 0)
+    blocks = tok.at[pl.ds(0, Z)]
+    rdma(blocks, blocks, pair_sent.at[0], ag_recv.at[0, 0], (f, partner)).wait_send()
+    if late:
+        @pl.when(end)
+        def _():
+            end_weights().wait_send()
+            for h in range(2):
+                end_hidden(h).wait_send()
+
+        @pl.when(near)
+        def _():
+            d2_sent()
+
+    def by_count(alls, step, total, skipped):
+        if not reuse:
+            if late:
+                @pl.when(end)
+                def _():
+                    alls(total - skipped).wait_send()
+
+                @pl.when(jnp.logical_not(end))
+                def _():
+                    alls(total).wait_send()
+            else:
+                alls(total).wait_send()
+        else:
+            for p in range(min(ring, total)):
+                if p < total - skipped or not late:
+                    step(p)
+                else:
+                    @pl.when(jnp.logical_not(end))
+                    def _():
+                        step(p)
+
+    def pair_step(p):
+        pair_copy(p, 0).wait_send()
+
+    def sum_step_sent(p):
+        for h in range(SPLIT):
+            sum_copy(p, h, 0, partner).wait_send()
+
+    by_count(pair_all, pair_step, Z * F, F)
+    lax.fori_loop(0, F, own_finish, 0)
+    by_count(sum_all, sum_step_sent, (Z - 1) * F, F)
 
 
 def place(H, S, wbuf, mix, o_mixed, o_eg, o_eu, o_ed, o_sg, o_su, o_sd, sems):
@@ -447,42 +659,51 @@
     Z = T // 2
     N, U = (Z - 1) * F, Z * F
     ring = min(U, RING)
+    HP = -(-(H + S) // 128) * 128
     bf, f32 = jnp.bfloat16, jnp.float32
     dma = pltpu.SemaphoreType.DMA
     wbuf, mix = pl.pallas_call(
         functools.partial(kernel, F, T, H, S, M),
         out_shape=[pltpu.VMEM((F, 3 * H + 3 * S, cw), bf), pltpu.VMEM((F, M, cw), bf)],
-        in_specs=[pl.BlockSpec(memory_space=pltpu.VMEM)] * 2
-        + [pl.BlockSpec(memory_space=pl.ANY)] * 6
-        + [pl.BlockSpec(memory_space=pltpu.VMEM)] * 2,
+        in_specs=[pl.BlockSpec(memory_space=pl.ANY)] * 10,
         out_specs=[pl.BlockSpec(memory_space=pltpu.VMEM)] * 2,
         scratch_shapes=[
             pltpu.VMEM((T, M, D), bf),
             pltpu.VMEM((T, T, M), f32),
-            pltpu.VMEM((T, M, H), bf),
-            pltpu.VMEM((T, M, S), bf),
+            pltpu.VMEM((T, M, HP), bf),
             pltpu.VMEM((F + 2 * SLOTS, M, cw), f32),
             pltpu.VMEM((ring, M, cw), bf),
             pltpu.VMEM((U, M, cw), bf),
             pltpu.VMEM((ring, M, cw), bf),
             pltpu.VMEM((F * (Z + 1), M, cw), bf),
-            dma((T, PARTS, 3)),
+            pltpu.VMEM((F, H + S, cw), bf),
+            pltpu.VMEM((2, M, HP), bf),
+            dma((T, 2)),
             dma((T, PARTS)),
-            dma((T,)),
-            dma((T,)),
-            dma((4, F)),
+            dma((1,)),
+            dma((1,)),
+            dma((1,)),
+            dma((2, F)),
             dma((4, F)),
             dma((ring,)),
             dma((U,)),
-            dma((ring,)),
-            dma((F * (Z + 1),)),
+            dma((ring, SPLIT)),
+            dma((F * (Z + 1), SPLIT)),
+            dma((2, F)),
+            dma((2, F)),
+            dma((3,)),
+            dma((3,)),
             pltpu.VMEM((H, cw), f32),
             pltpu.VMEM((H, cw), f32),
             pltpu.VMEM((H, cw), f32),
             pltpu.VMEM((S, cw), f32),
             pltpu.VMEM((S, cw), f32),
             pltpu.VMEM((S, cw), f32),
-            dma((6,)),
+            pltpu.VMEM((M, D), bf),
+            pltpu.VMEM((1, cw), f32),
+            pltpu.VMEM(routes.shape[::-1], jnp.int32),
+            pltpu.VMEM(route_weight.shape[::-1], f32),
+            dma((10,)),
         ],
         compiler_params=pltpu.CompilerParams(
             collective_id=0, has_side_effects=True, vmem_limit_bytes=VMEM_LIMIT

time: 77 us -> 71.9 us (0.934)
  Pallas kernels: 76.2 us -> 71.1 us
    pallas_call x1, Pallas kernels: 73.9 us -> 68.8 us  [local(): pl.pallas_call(functools.partial(kernel, F, T, H, S, M), out_shape=[pltpu...]
where the time goes in v3:
time: 71.9 us; the launch traced here: 71.8 us
  Pallas kernels  71.1 us (99%)
    pallas_call x1, Pallas kernels, local(): pl.pallas_call(functools.partial(kernel, F, T, H, S, M), out_shape=[pltpu...  68.8 us
    pallas_call x1, Pallas kernels, local(): pl.pallas_call(functools.partial(place, H, S), out_shape=[jax.ShapeDtypeS...  2.32 us

profile of v3, /device:TPU:0, one launch (start us, length us, event | category | flops | bytes accessed | tf_op | source)
XLA Modules:
  0.0 71.8 jit_solution(15981942819216804887)
XLA Ops:
  0.6 68.8 %shard_map.153 = (bf16[4,960,512]{2,1,0:T(8,128)(2,1)S(1)}, bf16[4,128,512]{2,1,0:T(8,128)(2,1)S(1)}) custom-call(bf16[128,2048]{1,0:T(8,128)(2,1)} %tokens.1, f32[1,512]{1,0:T(1,128)} %bitcast.12, f32[256,512]{1,0:T(8,128)} %bitcast.9, f32[256,512]{1,0:T(8,128)} %bitcast.10, f32[256,512]{1,0:T(8,128)} %bitcast.11, f32[64,512]{1,0:T(8,128)} %sh_gate.1, ...), custom_call_target="tpu_custom_call" | custom-call | tf_op jit(solution)/shard_map/pallas_call | solution.py:665
  69.5 2.3 %shard_map.154 = (bf16[128,2048]{1,0:T(8,128)(2,1)}, bf16[256,2048]{1,0:T(8,128)(2,1)}, bf16[256,2048]{1,0:T(8,128)(2,1)}, bf16[256,2048]{1,0:T(8,128)(2,1)}, bf...) custom-call(bf16[4,960,512]{2,1,0:T(8,128)(2,1)S(1)} %get-tuple-element.16.wbuf, ...), custom_call_target="tpu_custom_call" | custom-call | tf_op jit(solution)/shard_map/pallas_call | solution.py:715

commit v4 on v3

--- a/solution.py
+++ b/solution.py
@@ -12,7 +12,7 @@
 CONTRACT = (((1,), (1,)), ((), ()))
 MESH = pl.DeviceIdType.MESH
 PARTS = 4
-HELD = 2
+HELD = 1
 SPLIT = 4
 AHEAD = 1
 SLOTS = AHEAD + 2
@@ -28,7 +28,7 @@
     F, T, H, S, M,
     tokens, gain, ex_gate, ex_up, ex_down, sh_gate, sh_up, sh_down, routes, rweight,
     wbuf, mix,
-    tok, wt, hid, own, pout, pin, sout, sin, down2, hid2,
+    tok, wt, hid, own, pout, pin, sout, sin, down2, hid2, base,
     ag_send, ag_recv, pair_sent, wt_send, wt_recv, w_send, w_recv,
     pout_sem, pin_sem, sout_sem, sin_sem, d2_send, d2_recv, z_send, z_recv,
     l_eg, l_eu, l_ed, l_sg, l_su, l_sd, l_tok, l_gain, l_ids, l_rw, load_sem,
@@ -166,7 +166,8 @@
         return rdma(wbuf.at[f, GU:ALL, :], down2.at[f], z_send.at[0], z_recv.at[0], (f, inner))
 
     def end_hidden(h):
-        part = pl.ds(h * (rows // 2), rows // 2)
+        ready = (PARTS - HELD) * piece
+        part = pl.ds(0, ready) if h == 0 else pl.ds(ready, rows - ready)
         return rdma(
             hid.at[pl.ds(2 * (inner // 2), 2), part], hid2.at[:, part],
             z_send.at[1 + h], z_recv.at[1 + h], (f, inner),
@@ -295,6 +296,11 @@
         return carry
 
     if late:
+        @pl.when(end)
+        def _():
+            hidden_rows(inner // 2, range(PARTS - HELD))
+            end_hidden(0).start()
+
         lax.fori_loop(0, Z, early_step, 0)
     else:
         lax.fori_loop(0, Z, hidden_step, 0)
@@ -322,8 +328,10 @@
     def produce(o, j, d, done, extra=False):
         q = chunk(j)
         p = lax.rem(done, ring)
-        x = hid[pl.ds(2 * d, 2)].reshape(2 * rows, hid.shape[2])[:, 0:HS]
-        r = jnp.dot(x, wbuf[q, GU:ALL, :], preferred_element_type=jnp.float32)
+
+        def partial():
+            x = hid[pl.ds(2 * d, 2)].reshape(2 * rows, hid.shape[2])[:, 0:HS]
+            return jnp.dot(x, wbuf[q, GU:ALL, :], preferred_element_type=jnp.float32)
 
         if reuse:
             @pl.when(done >= ring)
@@ -334,19 +342,19 @@
             @pl.when(near)
             def _():
                 y = hid2[...].reshape(2 * rows, hid.shape[2])[:, 0:HS]
-                share(o, r + jnp.dot(y, down2[q], preferred_element_type=jnp.float32), p)
+                share(o, base[j] + jnp.dot(y, down2[q], preferred_element_type=jnp.float32), p)
 
             @pl.when(jnp.logical_not(near))
             def _():
-                share(o, r, p)
+                share(o, partial(), p)
         else:
-            share(o, r, p)
+            share(o, partial(), p)
         pair_copy(p, j * Z + d).start()
 
     def finish(o, j, d, sent):
         q = chunk(j)
         p = lax.rem(sent, ring)
-        base = j * (Z + 1)
+        first_slot = j * (Z + 1)
         pair_copy(0, j * Z + d).wait_recv()
         own[o] = own[o] + pin[j * Z + d].astype(jnp.float32)
         if late:
@@ -367,12 +375,12 @@
 
             @pl.when(from_left)
             def _():
-                sum_copy(0, h, base + d, me).wait_recv()
-                own[o, part] = own[o, part] + sin[base + d, part].astype(jnp.float32)
+                sum_copy(0, h, first_slot + d, me).wait_recv()
+                own[o, part] = own[o, part] + sin[first_slot + d, part].astype(jnp.float32)
 
             @pl.when(from_right)
             def _():
-                slot = base + jnp.where(d == z, Z, d)
+                slot = first_slot + jnp.where(d == z, Z, d)
                 sum_copy(0, h, slot, me).wait_recv()
                 own[o, part] = own[o, part] + sin[slot, part].astype(jnp.float32)
 
@@ -382,11 +390,11 @@
 
             @pl.when(d > z)
             def _():
-                sum_copy(p, h, base + d, right(me)).start()
+                sum_copy(p, h, first_slot + d, right(me)).start()
 
             @pl.when(d < z)
             def _():
-                sum_copy(p, h, base + jnp.where(d == z - 1, Z, d), left(me)).start()
+                sum_copy(p, h, first_slot + jnp.where(d == z - 1, Z, d), left(me)).start()
 
         @pl.when(d == z)
         def _():
@@ -418,7 +426,7 @@
             def _():
                 w_copy(1, lax.rem(f + j, F), 1, f).wait_recv()
 
-    steps = F + 1 + AHEAD
+    count = (Z - 2 if late else Z - 1) * F
     if square:
         bounds2 = (0, halves(HS), HS)
     else:
@@ -463,39 +471,59 @@
         for i in range(3) if square else range(1, F):
             rdma(down2.at[f], down2.at[f], d2_send.at[0, i], d2_recv.at[0, f], (fx if square else f, me)).wait_send()
 
+    def unit(n):
+        n = jnp.clip(n, 0, count - 1)
+        k = n // F
+        j = lax.rem(n, F)
+        if late:
+            second = (n >= F - 1) & (n < 2 * F - 1)
+            k = jnp.where(second, 1, jnp.where(n == 2 * F - 1, 0, k))
+            j = jnp.where(second, n - (F - 1), j)
+        return k, j
+
+    def own_base(j, carry):
+        x = hid[pl.ds(2 * z, 2)].reshape(2 * rows, hid.shape[2])[:, 0:HS]
+        base[j] = jnp.dot(x, wbuf[chunk(j), GU:ALL, :], preferred_element_type=jnp.float32)
+        return carry
+
     def sum_step(n, carry):
         done, sent = carry
-        k = n // steps
-        j = lax.rem(n, steps)
+        k, j = unit(n)
+        live = n < count
+
+        def finish_side(s, m, sent, allowed):
+            i, t = unit(m)
+            d, valid = side(i, s)
+            valid = valid & (m >= 0) & (m < count) & allowed
+
+            @pl.when(valid)
+            def _():
+                finish(F + SLOTS * s + lax.rem(jnp.maximum(m, 0), SLOTS), t, d, sent)
+
+            return sent + jnp.where(valid, 1, 0)
 
         if late:
-            @pl.when((n == steps) & end)
-            def _():
-                gather_step(Z - 1, 0)
+            sent = finish_side(0, n - 1, sent, end)
+
+            @pl.when((n == F - 1) & end)
+            def _():
                 if Z > 4:
                     lax.fori_loop(0, Z, rest_step, 0)
                 hidden_step(last, 0)
 
-            @pl.when((n == steps) & near)
+            @pl.when((n == F) & near)
             def _():
                 d2_pass()
 
-        if late:
-            d, valid = side(k, 0)
-            valid = valid & end & (k == 0) & (j > 0) & (j <= F)
-
-            @pl.when(valid)
-            def _():
-                finish(F + lax.rem(j + SLOTS - 1, SLOTS), j - 1, d, sent)
-
-            sent = sent + jnp.where(valid, 1, 0)
-
-            @pl.when((n == 1) & end)
-            def _():
-                hidden_rows(inner // 2, range(PARTS - HELD))
-                end_hidden(0).start()
-
-        @pl.when((k == 0) & (j < F))
+            @pl.when((n == 2 * F - 1) & near)
+            def _():
+                lax.fori_loop(0, F, own_base, 0)
+
+            fresh = ((k == 0) & (j < F - 1)) | ((k == 1) & (j == F - 1))
+        else:
+            fresh = k == 0
+
+        @pl.when(live & fresh)
         def _():
             down_weights(j)
 
@@ -506,28 +534,23 @@
 
         for s in range(2):
             d, valid = side(k, s)
-            valid = valid & (j < F)
+            valid = valid & live
 
             @pl.when(valid)
             def _():
-                produce(F + SLOTS * s + lax.rem(j, SLOTS), j, d, done)
+                produce(F + SLOTS * s + lax.rem(n, SLOTS), j, d, done)
 
             done = done + jnp.where(valid, 1, 0)
-        for s in range(2):
-            d, valid = side(k, s)
-            i = j - 1 - AHEAD * s
-            valid = valid & (i >= 0) & (i < F)
-            if late and s == 0:
-                valid = valid & jnp.logical_not(end & (k == 0))
-
-            @pl.when(valid)
-            def _():
-                finish(F + SLOTS * s + lax.rem(jnp.maximum(i, 0), SLOTS), i, d, sent)
-
-            sent = sent + jnp.where(valid, 1, 0)
+        if late:
+            @pl.when((n == F - 2) & end)
+            def _():
+                gather_step(Z - 1, 0)
+
+        sent = finish_side(0, n - 1, sent, jnp.logical_not(end) if late else True)
+        sent = finish_side(1, n - 1 - AHEAD, sent, True)
         return done, sent
 
-    done, sent = lax.fori_loop(0, (Z - 2 if late else Z - 1) * steps, sum_step, (0, 0))
+    done, sent = lax.fori_loop(0, count + 1 + AHEAD, sum_step, (0, 0))
     if late:
         @pl.when(end)
         def _():
@@ -678,18 +701,19 @@
             pltpu.VMEM((F * (Z + 1), M, cw), bf),
             pltpu.VMEM((F, H + S, cw), bf),
             pltpu.VMEM((2, M, HP), bf),
+            pltpu.VMEM((F, 2 * M, cw), f32),
             dma((T, 2)),
             dma((T, PARTS)),
             dma((1,)),
             dma((1,)),
             dma((1,)),
-            dma((2, F)),
-            dma((4, F)),
-            dma((ring,)),
+            dma((1, 3) if F == 4 else (2, F)),
+            dma((4, F) if F == 4 else (2, F)),
+            dma((ring if U > ring else 1,)),
             dma((U,)),
-            dma((ring, SPLIT)),
+            dma((ring, SPLIT) if U > ring else (1, 1)),
             dma((F * (Z + 1), SPLIT)),
-            dma((2, F)),
+            dma((1, F)),
             dma((2, F)),
             dma((3,)),
             dma((3,)),

time: 71.9 us -> 68.3 us (0.950)
  Pallas kernels: 71.1 us -> 67.5 us
    pallas_call x1, Pallas kernels: 68.8 us -> 65.2 us  [local(): pl.pallas_call(functools.partial(kernel, F, T, H, S, M), out_shape=[pltpu...]
where the time goes in v4:
time: 68.3 us; the launch traced here: 68.1 us
  Pallas kernels  67.5 us (99%)
    pallas_call x1, Pallas kernels, local(): pl.pallas_call(functools.partial(kernel, F, T, H, S, M), out_shape=[pltpu...  65.2 us
    pallas_call x1, Pallas kernels, local(): pl.pallas_call(functools.partial(place, H, S), out_shape=[jax.ShapeDtypeS...  2.32 us

profile of v4, /device:TPU:0, one launch (start us, length us, event | category | flops | bytes accessed | tf_op | source)
XLA Modules:
  0.0 68.1 jit_solution(4623674801697454174)
XLA Ops:
  0.6 65.2 %shard_map.153 = (bf16[4,960,512]{2,1,0:T(8,128)(2,1)S(1)}, bf16[4,128,512]{2,1,0:T(8,128)(2,1)S(1)}) custom-call(bf16[128,2048]{1,0:T(8,128)(2,1)} %tokens.1, f32[1,512]{1,0:T(1,128)} %bitcast.12, f32[256,512]{1,0:T(8,128)} %bitcast.9, f32[256,512]{1,0:T(8,128)} %bitcast.10, f32[256,512]{1,0:T(8,128)} %bitcast.11, f32[64,512]{1,0:T(8,128)} %sh_gate.1, ...), custom_call_target="tpu_custom_call" | custom-call | tf_op jit(solution)/shard_map/pallas_call | solution.py:688
  65.8 2.3 %shard_map.154 = (bf16[128,2048]{1,0:T(8,128)(2,1)}, bf16[256,2048]{1,0:T(8,128)(2,1)}, bf16[256,2048]{1,0:T(8,128)(2,1)}, bf16[256,2048]{1,0:T(8,128)(2,1)}, bf...) custom-call(bf16[4,960,512]{2,1,0:T(8,128)(2,1)S(1)} %get-tuple-element.16.wbuf, ...), custom_call_target="tpu_custom_call" | custom-call | tf_op jit(solution)/shard_map/pallas_call | solution.py:739

commit v5 on v4

--- a/solution.py
+++ b/solution.py
@@ -29,9 +29,9 @@
     tokens, gain, ex_gate, ex_up, ex_down, sh_gate, sh_up, sh_down, routes, rweight,
     wbuf, mix,
     tok, wt, hid, own, pout, pin, sout, sin, down2, hid2, base,
-    ag_send, ag_recv, pair_sent, wt_send, wt_recv, w_send, w_recv,
+    ag_send, ag_recv, wt_send, wt_recv, w_send, w_recv,
     pout_sem, pin_sem, sout_sem, sin_sem, d2_send, d2_recv, z_send, z_recv,
-    l_eg, l_eu, l_ed, l_sg, l_su, l_sd, l_tok, l_gain, l_ids, l_rw, load_sem,
+    l_w, l_tok, l_gain, l_ids, l_rw, load_sem,
 ):
     f = lax.axis_index("fs")
     me = lax.axis_index("tp")
@@ -59,12 +59,12 @@
         pl.semaphore_signal(barrier, inc=1, device_id=(lax.rem(f + i, F), me), device_id_type=MESH)
     for i in range(1, T):
         pl.semaphore_signal(barrier, inc=1, device_id=(f, lax.rem(me + i, T)), device_id_type=MESH)
+    parts = ((ex_gate, 0, H), (ex_up, H, H), (sh_gate, 2 * H, S), (sh_up, 2 * H + S, S), (ex_down, GU, H), (sh_down, GU + H, S))
     loads = [
         pltpu.make_async_copy(src, dst, load_sem.at[i])
-        for i, (src, dst) in enumerate((
-            (tokens, l_tok), (routes, l_ids), (rweight, l_rw), (gain, l_gain),
-            (ex_gate, l_eg), (ex_up, l_eu), (sh_gate, l_sg), (sh_up, l_su), (ex_down, l_ed), (sh_down, l_sd),
-        ))
+        for i, (src, dst) in enumerate(((tokens, l_tok), (routes, l_ids), (rweight, l_rw), (gain, l_gain)))
+    ] + [
+        pltpu.make_async_copy(src, l_w.at[lo:lo + n], load_sem.at[4 if lo < GU else 5]) for src, lo, n in parts
     ]
     for load in loads:
         load.start()
@@ -82,15 +82,10 @@
     for k in range(ids.shape[0]):
         comb = comb + jnp.where(expert == ids[k:k + 1, :], w[k:k + 1, :], 0.0)
     wt[me] = comb
-    for load in loads[4:]:
-        load.wait()
-    scale = l_gain[...]
-    wbuf[f, 0:H, :] = (l_eg[...] * scale).astype(jnp.bfloat16)
-    wbuf[f, H:2 * H, :] = (l_eu[...] * scale).astype(jnp.bfloat16)
-    wbuf[f, 2 * H:2 * H + S, :] = (l_sg[...] * scale).astype(jnp.bfloat16)
-    wbuf[f, 2 * H + S:GU, :] = (l_su[...] * scale).astype(jnp.bfloat16)
-    wbuf[f, GU:GU + H, :] = l_ed[...].astype(jnp.bfloat16)
-    wbuf[f, GU + H:ALL, :] = l_sd[...].astype(jnp.bfloat16)
+    pltpu.make_async_copy(l_w.at[0:GU], l_w.at[0:GU], load_sem.at[4]).wait()
+    wbuf[f, 0:GU, :] = (l_w[0:GU, :] * l_gain[...]).astype(jnp.bfloat16)
+    pltpu.make_async_copy(l_w.at[GU:ALL], l_w.at[GU:ALL], load_sem.at[5]).wait()
+    wbuf[f, GU:ALL, :] = l_w[GU:ALL, :].astype(jnp.bfloat16)
 
     pl.semaphore_wait(barrier, F - 1 + T - 1)
 
@@ -102,7 +97,7 @@
 
     def tok_copy(s, h, way, t):
         part = pl.ds(h * piece, piece)
-        sem = ag_send.at[s, way] if way < 2 else pair_sent.at[0]
+        sem = ag_send.at[way]
         return rdma(tok.at[s, part], tok.at[s, part], sem, ag_recv.at[s, h], (f, t))
 
     if square:
@@ -278,11 +273,11 @@
     def left_dest(k):
         return jnp.where(k < Z - 2, Z - 3 - k, Z - 2)
 
-    first = jnp.where(z == 0, Z - 1 - left_dest(0), left_dest(0))
+    first = jnp.where(2 * z < Z, Z - 1 - left_dest(0), left_dest(0))
     last = Z - 1 - z
 
-    def early_step(k, carry):
-        @pl.when((k == first) | jnp.logical_not(end))
+    def other_step(k, carry):
+        @pl.when(k != first)
         def _():
             hidden_step(k, carry)
 
@@ -301,7 +296,7 @@
             hidden_rows(inner // 2, range(PARTS - HELD))
             end_hidden(0).start()
 
-        lax.fori_loop(0, Z, early_step, 0)
+        hidden_step(first, 0)
     else:
         lax.fori_loop(0, Z, hidden_step, 0)
 
@@ -351,54 +346,52 @@
             share(o, partial(), p)
         pair_copy(p, j * Z + d).start()
 
-    def finish(o, j, d, sent):
-        q = chunk(j)
-        p = lax.rem(sent, ring)
-        first_slot = j * (Z + 1)
+    def begin(o, j, d, p):
         pair_copy(0, j * Z + d).wait_recv()
         own[o] = own[o] + pin[j * Z + d].astype(jnp.float32)
+        if reuse:
+            @pl.when((d != z) & (p >= ring))
+            def _():
+                for h in range(SPLIT):
+                    sum_copy(lax.rem(p, ring), h, 0, partner).wait_send()
+
+    def pass_piece(o, j, d, p, h):
+        p = lax.rem(p, ring)
+        first_slot = j * (Z + 1)
         if late:
             from_left = (z > 0) & ((d > z) | ((d == z) & (z > 1)))
             from_right = (z < Z - 1) & ((d < z) | ((d == z) & (z < Z - 2)))
         else:
             from_left = (d >= z) & (z > 0)
             from_right = (d <= z) & (z < Z - 1)
-
-        if reuse:
-            @pl.when((d != z) & (sent >= ring))
-            def _():
-                for h in range(SPLIT):
-                    sum_copy(p, h, 0, partner).wait_send()
-
-        for h in range(SPLIT):
-            part = pl.ds(h * strip, strip)
-
-            @pl.when(from_left)
-            def _():
-                sum_copy(0, h, first_slot + d, me).wait_recv()
-                own[o, part] = own[o, part] + sin[first_slot + d, part].astype(jnp.float32)
-
-            @pl.when(from_right)
-            def _():
-                slot = first_slot + jnp.where(d == z, Z, d)
-                sum_copy(0, h, slot, me).wait_recv()
-                own[o, part] = own[o, part] + sin[slot, part].astype(jnp.float32)
-
-            @pl.when(d != z)
-            def _():
-                sout[p, part] = own[o, part].astype(jnp.bfloat16)
-
-            @pl.when(d > z)
-            def _():
-                sum_copy(p, h, first_slot + d, right(me)).start()
-
-            @pl.when(d < z)
-            def _():
-                sum_copy(p, h, first_slot + jnp.where(d == z - 1, Z, d), left(me)).start()
+        part = pl.ds(h * strip, strip)
+
+        @pl.when(from_left)
+        def _():
+            sum_copy(0, h, first_slot + d, me).wait_recv()
+            own[o, part] = own[o, part] + sin[first_slot + d, part].astype(jnp.float32)
+
+        @pl.when(from_right)
+        def _():
+            slot = first_slot + jnp.where(d == z, Z, d)
+            sum_copy(0, h, slot, me).wait_recv()
+            own[o, part] = own[o, part] + sin[slot, part].astype(jnp.float32)
+
+        @pl.when(d != z)
+        def _():
+            sout[p, part] = own[o, part].astype(jnp.bfloat16)
+
+        @pl.when(d > z)
+        def _():
+            sum_copy(p, h, first_slot + d, right(me)).start()
+
+        @pl.when(d < z)
+        def _():
+            sum_copy(p, h, first_slot + jnp.where(d == z - 1, Z, d), left(me)).start()
 
         @pl.when(d == z)
         def _():
-            mix[q] = own[o].astype(jnp.bfloat16)
+            mix[chunk(j), part] = own[o, part].astype(jnp.bfloat16)
 
     def side(k, s):
         d = left_dest(k)
@@ -481,43 +474,64 @@
             j = jnp.where(second, n - (F - 1), j)
         return k, j
 
-    def own_base(j, carry):
+    def own_base(j):
         x = hid[pl.ds(2 * z, 2)].reshape(2 * rows, hid.shape[2])[:, 0:HS]
         base[j] = jnp.dot(x, wbuf[chunk(j), GU:ALL, :], preferred_element_type=jnp.float32)
-        return carry
 
     def sum_step(n, carry):
         done, sent = carry
         k, j = unit(n)
         live = n < count
 
-        def finish_side(s, m, sent, allowed):
+        if late:
+            @pl.when((n == 1) & jnp.logical_not(end))
+            def _():
+                lax.fori_loop(0, Z, other_step, 0)
+
+        def going(s, m, p):
             i, t = unit(m)
             d, valid = side(i, s)
-            valid = valid & (m >= 0) & (m < count) & allowed
-
+            valid = valid & (m >= 0) & (m < count)
+            return F + SLOTS * s + lax.rem(jnp.maximum(m, 0), SLOTS), t, d, p, valid
+
+        flows = [going(0, n - 1, sent)]
+        flows.append(going(1, n - 1 - AHEAD, sent + jnp.where(flows[0][4], 1, 0)))
+        sent = flows[1][3] + jnp.where(flows[1][4], 1, 0)
+        for o, t, d, p, valid in flows:
             @pl.when(valid)
             def _():
-                finish(F + SLOTS * s + lax.rem(jnp.maximum(m, 0), SLOTS), t, d, sent)
-
-            return sent + jnp.where(valid, 1, 0)
-
+                begin(o, t, d, p)
+
+        def pieces(parts, allowed):
+            for h in parts:
+                for o, t, d, p, valid in flows:
+                    @pl.when(valid & allowed)
+                    def _():
+                        pass_piece(o, t, d, p, h)
+
+        def start(s, done):
+            d, valid = side(k, s)
+            valid = valid & live
+
+            @pl.when(valid)
+            def _():
+                produce(F + SLOTS * s + lax.rem(n, SLOTS), j, d, done)
+
+            return done + jnp.where(valid, 1, 0)
+
+        middle = jnp.logical_not(end)
+        pieces(range(SPLIT // 2), True)
+        pieces(range(SPLIT // 2, SPLIT), end)
         if late:
-            sent = finish_side(0, n - 1, sent, end)
-
             @pl.when((n == F - 1) & end)
             def _():
                 if Z > 4:
                     lax.fori_loop(0, Z, rest_step, 0)
                 hidden_step(last, 0)
 
-            @pl.when((n == F) & near)
+            @pl.when((n == F + 1) & near)
             def _():
                 d2_pass()
-
-            @pl.when((n == 2 * F - 1) & near)
-            def _():
-                lax.fori_loop(0, F, own_base, 0)
 
             fresh = ((k == 0) & (j < F - 1)) | ((k == 1) & (j == F - 1))
         else:
@@ -532,22 +546,22 @@
             def _():
                 d2_own()
 
-        for s in range(2):
-            d, valid = side(k, s)
-            valid = valid & live
-
-            @pl.when(valid)
-            def _():
-                produce(F + SLOTS * s + lax.rem(n, SLOTS), j, d, done)
-
-            done = done + jnp.where(valid, 1, 0)
+        done = start(0, done)
+        pieces(range(SPLIT // 2, SPLIT - 1), middle)
+        done = start(1, done)
+        if late:
+            b = jnp.where(n == 2 * F - 1, F - 1, n - 3)
+
+            @pl.when(near & (n > 2) & ((n < F + 2) | (n == 2 * F - 1)))
+            def _():
+                own_base(b)
+
+        pieces(range(SPLIT - 1, SPLIT), middle)
         if late:
             @pl.when((n == F - 2) & end)
             def _():
                 gather_step(Z - 1, 0)
 
-        sent = finish_side(0, n - 1, sent, jnp.logical_not(end) if late else True)
-        sent = finish_side(1, n - 1 - AHEAD, sent, True)
         return done, sent
 
     done, sent = lax.fori_loop(0, count + 1 + AHEAD, sum_step, (0, 0))
@@ -572,7 +586,9 @@
         return done + 1
 
     def own_finish(j, carry):
-        finish(j, j, z, sent)
+        begin(j, j, z, sent)
+        for h in range(SPLIT):
+            pass_piece(j, j, z, sent, h)
         return carry
 
     done = lax.fori_loop(0, F, own_produce, done)
@@ -593,25 +609,19 @@
             w_copy(1, f, i, lax.rem(f + i, F)).wait_send()
     wt_all().wait_send()
 
-    def block_sent(s, way, t):
-        return rdma(tok.at[s], tok.at[s], ag_send.at[s, way], ag_recv.at[s, 0], (f, t))
-
-    def drain(k, carry):
-        s = 2 * k + c
-
-        @pl.when((k <= z) & (z < Z - 1))
-        def _():
-            block_sent(s, 0, right(me)).wait_send()
-
-        @pl.when((k >= z) & (z > 0))
-        def _():
-            block_sent(s, 1, left(me)).wait_send()
-
-        return carry
-
-    lax.fori_loop(0, Z, drain, 0)
-    blocks = tok.at[pl.ds(0, Z)]
-    rdma(blocks, blocks, pair_sent.at[0], ag_recv.at[0, 0], (f, partner)).wait_send()
+    def blocks_sent(way, n):
+        blocks = tok.at[pl.ds(0, n)]
+        rdma(blocks, blocks, ag_send.at[way], ag_recv.at[0, 0], (f, partner)).wait_send()
+
+    for i in range(Z):
+        @pl.when(z == i)
+        def _():
+            if i < Z - 1:
+                blocks_sent(0, i + 1)
+            if i > 0:
+                blocks_sent(1, Z - i)
+
+    blocks_sent(2, Z)
     if late:
         @pl.when(end)
         def _():
@@ -651,8 +661,8 @@
         for h in range(SPLIT):
             sum_copy(p, h, 0, partner).wait_send()
 
+    lax.fori_loop(0, F, own_finish, 0)
     by_count(pair_all, pair_step, Z * F, F)
-    lax.fori_loop(0, F, own_finish, 0)
     by_count(sum_all, sum_step_sent, (Z - 1) * F, F)
 
 
@@ -661,17 +671,17 @@
     GU = 2 * H + 2 * S
     pieces = ((o_eg, 0, H), (o_eu, H, H), (o_ed, GU, H), (o_sg, 2 * H, S), (o_su, 2 * H + S, S), (o_sd, GU + H, S))
     copies = []
-    for p, (ref, lo, size) in enumerate(pieces):
+    for ref, lo, size in pieces:
         for q in range(F):
             copies.append(pltpu.make_async_copy(
-                wbuf.at[q, lo:lo + size, :], ref.at[:, q * cw:(q + 1) * cw], sems.at[p, q]
+                wbuf.at[q, lo:lo + size, :], ref.at[:, q * cw:(q + 1) * cw], sems.at[0]
             ))
     for q in range(F):
-        copies.append(pltpu.make_async_copy(mix.at[q], o_mixed.at[:, q * cw:(q + 1) * cw], sems.at[6, q]))
+        copies.append(pltpu.make_async_copy(mix.at[q], o_mixed.at[:, q * cw:(q + 1) * cw], sems.at[1]))
     for copy in copies:
         copy.start()
-    for copy in copies:
-        copy.wait()
+    pltpu.make_async_copy(wbuf, wbuf, sems.at[0]).wait()
+    pltpu.make_async_copy(mix, mix, sems.at[1]).wait()
 
 
 def local(F, T, tokens, gain, ex_gate, ex_up, ex_down, sh_gate, sh_up, sh_down, routes, route_weight):
@@ -702,9 +712,8 @@
             pltpu.VMEM((F, H + S, cw), bf),
             pltpu.VMEM((2, M, HP), bf),
             pltpu.VMEM((F, 2 * M, cw), f32),
-            dma((T, 2)),
+            dma((3,)),
             dma((T, PARTS)),
-            dma((1,)),
             dma((1,)),
             dma((1,)),
             dma((1, 3) if F == 4 else (2, F)),
@@ -717,17 +726,12 @@
             dma((2, F)),
             dma((3,)),
             dma((3,)),
-            pltpu.VMEM((H, cw), f32),
-            pltpu.VMEM((H, cw), f32),
-            pltpu.VMEM((H, cw), f32),
-            pltpu.VMEM((S, cw), f32),
-            pltpu.VMEM((S, cw), f32),
-            pltpu.VMEM((S, cw), f32),
+            pltpu.VMEM((3 * H + 3 * S, cw), f32),
             pltpu.VMEM((M, D), bf),
             pltpu.VMEM((1, cw), f32),
             pltpu.VMEM(routes.shape[::-1], jnp.int32),
             pltpu.VMEM(route_weight.shape[::-1], f32),
-            dma((10,)),
+            dma((6,)),
         ],
         compiler_params=pltpu.CompilerParams(
             collective_id=0, has_side_effects=True, vmem_limit_bytes=VMEM_LIMIT
@@ -743,7 +747,7 @@
         + [jax.ShapeDtypeStruct((S, D), bf)] * 3,
         in_specs=[pl.BlockSpec(memory_space=pltpu.VMEM)] * 2,
         out_specs=[pl.BlockSpec(memory_space=pl.ANY)] * 7,
-        scratch_shapes=[dma((7, F))],
+        scratch_shapes=[dma((2,))],
         compiler_params=pltpu.CompilerParams(vmem_limit_bytes=4 << 20),
     )(pltpu.with_memory_space_constraint(wbuf, pltpu.VMEM), pltpu.with_memory_space_constraint(mix, pltpu.VMEM))
     return (mixed, eg[None], eu[None], ed[None], sg, su, sd)

time: 68.3 us -> 67 us (0.981)
  Pallas kernels: 67.5 us -> 66.2 us
    pallas_call x1, Pallas kernels: 65.2 us -> 64.1 us  [local(): pl.pallas_call(functools.partial(kernel, F, T, H, S, M), out_shape=[pltpu...]
where the time goes in v5:
time: 67 us; the launch traced here: 66.9 us
  Pallas kernels  66.2 us (99%)
    pallas_call x1, Pallas kernels, local(): pl.pallas_call(functools.partial(kernel, F, T, H, S, M), out_shape=[pltpu...  64.1 us
    pallas_call x1, Pallas kernels, local(): pl.pallas_call(functools.partial(place, H, S), out_shape=[jax.ShapeDtypeS...  2.08 us

profile of v5, /device:TPU:0, one launch (start us, length us, event | category | flops | bytes accessed | tf_op | source)
XLA Modules:
  0.0 66.9 jit_solution(9604986200512319733)
XLA Ops:
  0.6 64.1 %shard_map.153 = (bf16[4,960,512]{2,1,0:T(8,128)(2,1)S(1)}, bf16[4,128,512]{2,1,0:T(8,128)(2,1)S(1)}) custom-call(bf16[128,2048]{1,0:T(8,128)(2,1)} %tokens.1, f32[1,512]{1,0:T(1,128)} %bitcast.12, f32[256,512]{1,0:T(8,128)} %bitcast.9, f32[256,512]{1,0:T(8,128)} %bitcast.10, f32[256,512]{1,0:T(8,128)} %bitcast.11, f32[64,512]{1,0:T(8,128)} %sh_gate.1, ...), custom_call_target="tpu_custom_call" | custom-call | tf_op jit(solution)/shard_map/pallas_call | solution.py:698
  64.8 2.1 %shard_map.154 = (bf16[128,2048]{1,0:T(8,128)(2,1)}, bf16[256,2048]{1,0:T(8,128)(2,1)}, bf16[256,2048]{1,0:T(8,128)(2,1)}, bf16[256,2048]{1,0:T(8,128)(2,1)}, bf...) custom-call(bf16[4,960,512]{2,1,0:T(8,128)(2,1)S(1)} %get-tuple-element.16.wbuf, ...), custom_call_target="tpu_custom_call" | custom-call | tf_op jit(solution)/shard_map/pallas_call | solution.py:743

commit v6 on v5

--- a/solution.py
+++ b/solution.py
@@ -12,10 +12,10 @@
 CONTRACT = (((1,), (1,)), ((), ()))
 MESH = pl.DeviceIdType.MESH
 PARTS = 4
-HELD = 1
+HELD = 2
 SPLIT = 4
 AHEAD = 1
-SLOTS = AHEAD + 2
+SLOTS = AHEAD + 3
 RING = 16
 VMEM_LIMIT = 56 << 20
 
@@ -28,9 +28,9 @@
     F, T, H, S, M,
     tokens, gain, ex_gate, ex_up, ex_down, sh_gate, sh_up, sh_down, routes, rweight,
     wbuf, mix,
-    tok, wt, hid, own, pout, pin, sout, sin, down2, hid2, base,
+    tok, wt, hid, own, pout, pin, sout, sin, down2, hid2,
     ag_send, ag_recv, wt_send, wt_recv, w_send, w_recv,
-    pout_sem, pin_sem, sout_sem, sin_sem, d2_send, d2_recv, z_send, z_recv,
+    pout_sem, pin_sem, sout_sem, sin_sem, d2_send, d2_recv, d2_pair, z_send, z_recv,
     l_w, l_tok, l_gain, l_ids, l_rw, load_sem,
 ):
     f = lax.axis_index("fs")
@@ -51,6 +51,7 @@
     late = Z >= 4
     HS = H + S
     strip = rows // SPLIT
+    side_cols = cw // 2
     end = (z == 0) | (z == Z - 1)
     near = (z == 1) | (z == Z - 2)
 
@@ -101,14 +102,17 @@
         return rdma(tok.at[s, part], tok.at[s, part], sem, ag_recv.at[s, h], (f, t))
 
     if square:
-        bounds = (0, halves(GU), GU, GU + halves(ALL - GU), ALL)
+        bounds = (0, halves(GU), GU)
     else:
         bounds = (0, GU, ALL)
 
     def w_copy(part, src, i, peer):
-        lo, hi = bounds[part], bounds[part + 1]
+        if square and part >= 2:
+            block = wbuf.at[src, GU:ALL, (part - 2) * side_cols:(part - 1) * side_cols]
+        else:
+            block = wbuf.at[src, bounds[part]:bounds[part + 1], :]
         return rdma(
-            wbuf.at[src, lo:hi, :], wbuf.at[src, lo:hi, :],
+            block, block,
             w_send.at[0 if square else part, i], w_recv.at[part, src], (peer, me),
         )
 
@@ -158,15 +162,20 @@
     inner = jnp.where(z == 0, me + 2, jnp.where(z == Z - 1, me - 2, partner))
 
     def end_weights():
-        return rdma(wbuf.at[f, GU:ALL, :], down2.at[f], z_send.at[0], z_recv.at[0], (f, inner))
-
-    def end_hidden(h):
+        return rdma(wbuf.at[f, GU:ALL, :], down2.at[c, f], z_send.at[0], z_recv.at[0], (f, inner))
+
+    def end_hidden(h, core, sender):
         ready = (PARTS - HELD) * piece
         part = pl.ds(0, ready) if h == 0 else pl.ds(ready, rows - ready)
+        t = 2 * (inner // 2) + core
         return rdma(
-            hid.at[pl.ds(2 * (inner // 2), 2), part], hid2.at[:, part],
-            z_send.at[1 + h], z_recv.at[1 + h], (f, inner),
+            hid.at[t, part], hid2.at[sender, part],
+            z_send.at[1 + 2 * h + core], z_recv.at[1 + 2 * h + sender], (f, t),
         )
+
+    def send_hidden(h):
+        for core in range(2):
+            end_hidden(h, core, c).start()
 
     if late:
         @pl.when(end)
@@ -277,7 +286,7 @@
     last = Z - 1 - z
 
     def other_step(k, carry):
-        @pl.when(k != first)
+        @pl.when((k != first) & (k != z))
         def _():
             hidden_step(k, carry)
 
@@ -294,7 +303,7 @@
         @pl.when(end)
         def _():
             hidden_rows(inner // 2, range(PARTS - HELD))
-            end_hidden(0).start()
+            send_hidden(0)
 
         hidden_step(first, 0)
     else:
@@ -303,10 +312,17 @@
     ring = pout.shape[0]
     reuse = Z * F > ring
 
-    def chunk(j):
+    def chunks(j):
         if square:
-            return jnp.where(j == 0, f, jnp.where(j == 1, fx, jnp.where(j == 2, fy, fd)))
-        return lax.rem(f + j, F)
+            low = jnp.where(j == 0, f, jnp.where(j == 1, fy, jnp.where(j == 2, fx, fd)))
+            high = jnp.where(j == 0, f, jnp.where(j == 1, fx, jnp.where(j == 2, fy, fd)))
+            return (low, slice(0, side_cols)), (high, slice(side_cols, cw))
+        return ((lax.rem(f + j, F), slice(0, cw)),)
+
+    def down(x, j, block):
+        return jnp.concatenate(
+            [jnp.dot(x, block(q, cols), preferred_element_type=jnp.float32) for q, cols in chunks(j)], axis=1
+        )
 
     def pair_copy(p, slot):
         return rdma(pout.at[p], pin.at[slot], pout_sem.at[p if reuse else 0], pin_sem.at[slot], (f, partner))
@@ -320,30 +336,17 @@
         own[o] = jnp.where(c == 0, top, bottom)
         pout[p] = jnp.where(c == 0, bottom, top).astype(jnp.bfloat16)
 
-    def produce(o, j, d, done, extra=False):
-        q = chunk(j)
+    def produce(o, j, d, done):
         p = lax.rem(done, ring)
-
-        def partial():
-            x = hid[pl.ds(2 * d, 2)].reshape(2 * rows, hid.shape[2])[:, 0:HS]
-            return jnp.dot(x, wbuf[q, GU:ALL, :], preferred_element_type=jnp.float32)
+        x = hid[pl.ds(2 * d, 2)].reshape(2 * rows, hid.shape[2])[:, 0:HS]
+        r = down(x, j, lambda q, cols: wbuf[q, GU:ALL, cols])
 
         if reuse:
             @pl.when(done >= ring)
             def _():
                 pair_copy(p, 0).wait_send()
 
-        if extra:
-            @pl.when(near)
-            def _():
-                y = hid2[...].reshape(2 * rows, hid.shape[2])[:, 0:HS]
-                share(o, base[j] + jnp.dot(y, down2[q], preferred_element_type=jnp.float32), p)
-
-            @pl.when(jnp.logical_not(near))
-            def _():
-                share(o, partial(), p)
-        else:
-            share(o, partial(), p)
+        share(o, r, p)
         pair_copy(p, j * Z + d).start()
 
     def begin(o, j, d, p):
@@ -391,7 +394,8 @@
 
         @pl.when(d == z)
         def _():
-            mix[chunk(j), part] = own[o, part].astype(jnp.bfloat16)
+            for q, cols in chunks(j):
+                mix[q, part, cols] = own[o, part, cols].astype(jnp.bfloat16)
 
     def side(k, s):
         d = left_dest(k)
@@ -404,10 +408,10 @@
             @pl.when(j == 1)
             def _():
                 pass_weights(2, 3)
+
+            @pl.when(j == 2)
+            def _():
                 w_copy(2, fx, 0, fx).wait_recv()
-
-            @pl.when(j == 2)
-            def _():
                 w_copy(3, fy, 1, fy).wait_recv()
 
             @pl.when(j == 3)
@@ -428,9 +432,13 @@
     def d2_copy(part, src, i, peer):
         lo, hi = bounds2[part], bounds2[part + 1]
         return rdma(
-            down2.at[src, lo:hi, :], down2.at[src, lo:hi, :],
+            down2.at[c, src, lo:hi, :], down2.at[c, src, lo:hi, :],
             d2_send.at[0, i], d2_recv.at[part, src], (peer, me),
         )
+
+    def d2_share(src):
+        block = down2.at[c, src]
+        return rdma(block, block, d2_pair.at[0], d2_pair.at[1], (f, partner))
 
     def d2_own():
         end_weights().wait_recv()
@@ -442,6 +450,7 @@
         else:
             for i in range(1, F):
                 d2_copy(0, f, i, lax.rem(f + i, F)).start()
+        d2_share(f).start()
 
     def d2_pass():
         if square:
@@ -450,19 +459,31 @@
             d2_copy(1, fx, 0, fx).wait_recv()
             d2_copy(1, fx, 2, fy).start()
 
-    def d2_rest():
+    def d2_rest(i):
         if square:
-            d2_copy(0, fx, 0, fx).wait_recv()
-            d2_copy(1, fy, 1, fy).wait_recv()
-            d2_copy(0, fd, 2, fx).wait_recv()
-            d2_copy(1, fd, 2, fy).wait_recv()
-        else:
-            for i in range(1, F):
-                d2_copy(0, lax.rem(f + F - i, F), i, f).wait_recv()
+            if i == 0:
+                d2_copy(0, fx, 0, fx).wait_recv()
+                d2_share(fx).start()
+            elif i == 1:
+                d2_copy(1, fy, 1, fy).wait_recv()
+                d2_share(fy).start()
+            else:
+                d2_copy(0, fd, 2, fx).wait_recv()
+                d2_copy(1, fd, 2, fy).wait_recv()
+                d2_share(fd).start()
+        elif i == 2:
+            for t in range(1, F):
+                d2_copy(0, lax.rem(f + F - t, F), t, f).wait_recv()
+                d2_share(lax.rem(f + F - t, F)).start()
+
+    def d2_all(core):
+        block = down2.at[core]
+        return rdma(block, block, d2_pair.at[0], d2_pair.at[1], (f, partner))
 
     def d2_sent():
         for i in range(3) if square else range(1, F):
-            rdma(down2.at[f], down2.at[f], d2_send.at[0, i], d2_recv.at[0, f], (fx if square else f, me)).wait_send()
+            rdma(down2.at[c, f], down2.at[c, f], d2_send.at[0, i], d2_recv.at[0, f], (fx if square else f, me)).wait_send()
+        d2_all(c).wait_send()
 
     def unit(n):
         n = jnp.clip(n, 0, count - 1)
@@ -474,10 +495,6 @@
             j = jnp.where(second, n - (F - 1), j)
         return k, j
 
-    def own_base(j):
-        x = hid[pl.ds(2 * z, 2)].reshape(2 * rows, hid.shape[2])[:, 0:HS]
-        base[j] = jnp.dot(x, wbuf[chunk(j), GU:ALL, :], preferred_element_type=jnp.float32)
-
     def sum_step(n, carry):
         done, sent = carry
         k, j = unit(n)
@@ -494,8 +511,9 @@
             valid = valid & (m >= 0) & (m < count)
             return F + SLOTS * s + lax.rem(jnp.maximum(m, 0), SLOTS), t, d, p, valid
 
-        flows = [going(0, n - 1, sent)]
-        flows.append(going(1, n - 1 - AHEAD, sent + jnp.where(flows[0][4], 1, 0)))
+        m = n - 1 - jnp.where(end, 0, 1) if late else n - 2
+        flows = [going(0, m, sent)]
+        flows.append(going(1, m - AHEAD, sent + jnp.where(flows[0][4], 1, 0)))
         sent = flows[1][3] + jnp.where(flows[1][4], 1, 0)
         for o, t, d, p, valid in flows:
             @pl.when(valid)
@@ -533,6 +551,12 @@
             def _():
                 d2_pass()
 
+            for i in range(3):
+                @pl.when((n == F + 2 + i) & near)
+                def _():
+                    d2_rest(i)
+
+
             fresh = ((k == 0) & (j < F - 1)) | ((k == 1) & (j == F - 1))
         else:
             fresh = k == 0
@@ -551,47 +575,62 @@
         done = start(1, done)
         if late:
             b = jnp.where(n == 2 * F - 1, F - 1, n - 3)
-
-            @pl.when(near & (n > 2) & ((n < F + 2) | (n == 2 * F - 1)))
-            def _():
-                own_base(b)
+            turn = near & (n > 2) & ((n < F + 2) | (n == 2 * F - 1))
+
+            @pl.when(turn)
+            def _():
+                produce(b, b, z, done)
+
+            done = done + jnp.where(turn, 1, 0)
 
         pieces(range(SPLIT - 1, SPLIT), middle)
         if late:
+            @pl.when((n == 2) & middle)
+            def _():
+                hidden_step(z, 0)
+
             @pl.when((n == F - 2) & end)
             def _():
                 gather_step(Z - 1, 0)
 
         return done, sent
 
-    done, sent = lax.fori_loop(0, count + 1 + AHEAD, sum_step, (0, 0))
+    done, sent = lax.fori_loop(0, count + 2 + AHEAD, sum_step, (0, 0))
     if late:
         @pl.when(end)
         def _():
             for h in range(PARTS - HELD, PARTS):
                 gather_piece(1, h)
             hidden_rows(inner // 2, range(PARTS - HELD, PARTS))
-            end_hidden(1).start()
+            send_hidden(1)
             if Z == 4:
                 hidden_step(z, 0)
 
-        @pl.when(near)
-        def _():
-            d2_rest()
-            for h in range(2):
-                end_hidden(h).wait_recv()
-
     def own_produce(j, done):
-        produce(j, j, z, done, late)
+        produce(j, j, z, done)
         return done + 1
 
     def own_finish(j, carry):
         begin(j, j, z, sent)
+        if late:
+            @pl.when(near)
+            def _():
+                r = own[j]
+                for s in range(2):
+                    r = r + down(hid2[s][:, 0:HS], j, lambda q, cols: down2[s, q, :, cols])
+                own[j] = r
+
         for h in range(SPLIT):
             pass_piece(j, j, z, sent, h)
         return carry
 
-    done = lax.fori_loop(0, F, own_produce, done)
+    if late:
+        @pl.when(jnp.logical_not(near))
+        def _():
+            lax.fori_loop(0, F, own_produce, done)
+    else:
+        lax.fori_loop(0, F, own_produce, done)
+
     def pair_all(n):
         src, dst = pout.at[pl.ds(0, n)], pin.at[pl.ds(0, n)]
         return rdma(src, dst, pout_sem.at[0], pin_sem.at[0], (f, partner))
@@ -627,7 +666,8 @@
         def _():
             end_weights().wait_send()
             for h in range(2):
-                end_hidden(h).wait_send()
+                for core in range(2):
+                    end_hidden(h, core, c).wait_send()
 
         @pl.when(near)
         def _():
@@ -660,6 +700,14 @@
     def sum_step_sent(p):
         for h in range(SPLIT):
             sum_copy(p, h, 0, partner).wait_send()
+
+    if late:
+        @pl.when(near)
+        def _():
+            d2_all(1 - c).wait_recv()
+            for h in range(2):
+                for sender in range(2):
+                    end_hidden(h, 0, sender).wait_recv()
 
     lax.fori_loop(0, F, own_finish, 0)
     by_count(pair_all, pair_step, Z * F, F)
@@ -709,9 +757,8 @@
             pltpu.VMEM((U, M, cw), bf),
             pltpu.VMEM((ring, M, cw), bf),
             pltpu.VMEM((F * (Z + 1), M, cw), bf),
-            pltpu.VMEM((F, H + S, cw), bf),
+            pltpu.VMEM((2, F, H + S, cw), bf),
             pltpu.VMEM((2, M, HP), bf),
-            pltpu.VMEM((F, 2 * M, cw), f32),
             dma((3,)),
             dma((T, PARTS)),
             dma((1,)),
@@ -724,8 +771,9 @@
             dma((F * (Z + 1), SPLIT)),
             dma((1, F)),
             dma((2, F)),
-            dma((3,)),
-            dma((3,)),
+            dma((2,)),
+            dma((5,)),
+            dma((5,)),
             pltpu.VMEM((3 * H + 3 * S, cw), f32),
             pltpu.VMEM((M, D), bf),
             pltpu.VMEM((1, cw), f32),

time: 67 us -> 65.5 us (0.978)
  Pallas kernels: 66.2 us -> 64.7 us
    pallas_call x1, Pallas kernels: 64.1 us -> 62.7 us  [local(): pl.pallas_call(functools.partial(kernel, F, T, H, S, M), out_shape=[pltpu...]
where the time goes in v6:
time: 65.5 us; the launch traced here: 65.4 us
  Pallas kernels  64.7 us (99%)
    pallas_call x1, Pallas kernels, local(): pl.pallas_call(functools.partial(kernel, F, T, H, S, M), out_shape=[pltpu...  62.7 us
    pallas_call x1, Pallas kernels, local(): pl.pallas_call(functools.partial(place, H, S), out_shape=[jax.ShapeDtypeS...  2.08 us

profile of v6, /device:TPU:0, one launch (start us, length us, event | category | flops | bytes accessed | tf_op | source)
XLA Modules:
  0.0 65.4 jit_solution(7969002220027357751)
XLA Ops:
  0.6 62.7 %shard_map.153 = (bf16[4,960,512]{2,1,0:T(8,128)(2,1)S(1)}, bf16[4,128,512]{2,1,0:T(8,128)(2,1)S(1)}) custom-call(bf16[128,2048]{1,0:T(8,128)(2,1)} %tokens.1, f32[1,512]{1,0:T(1,128)} %bitcast.12, f32[256,512]{1,0:T(8,128)} %bitcast.9, f32[256,512]{1,0:T(8,128)} %bitcast.10, f32[256,512]{1,0:T(8,128)} %bitcast.11, f32[64,512]{1,0:T(8,128)} %sh_gate.1, ...), custom_call_target="tpu_custom_call" | custom-call | tf_op jit(solution)/shard_map/pallas_call | solution.py:746
  63.3 2.1 %shard_map.154 = (bf16[128,2048]{1,0:T(8,128)(2,1)}, bf16[256,2048]{1,0:T(8,128)(2,1)}, bf16[256,2048]{1,0:T(8,128)(2,1)}, bf16[256,2048]{1,0:T(8,128)(2,1)}, bf...) custom-call(bf16[4,960,512]{2,1,0:T(8,128)(2,1)S(1)} %get-tuple-element.16.wbuf, ...), custom_call_target="tpu_custom_call" | custom-call | tf_op jit(solution)/shard_map/pallas_call | solution.py:791

commit v7 on v6

--- a/solution.py
+++ b/solution.py
@@ -28,7 +28,7 @@
     F, T, H, S, M,
     tokens, gain, ex_gate, ex_up, ex_down, sh_gate, sh_up, sh_down, routes, rweight,
     wbuf, mix,
-    tok, wt, hid, own, pout, pin, sout, sin, down2, hid2,
+    tok, wt, hid, own, pout, pin, sout, sin, down2, hid2, pre,
     ag_send, ag_recv, wt_send, wt_recv, w_send, w_recv,
     pout_sem, pin_sem, sout_sem, sin_sem, d2_send, d2_recv, d2_pair, z_send, z_recv,
     l_w, l_tok, l_gain, l_ids, l_rw, load_sem,
@@ -242,9 +242,31 @@
                 tok_copy(me, h, 1, left(me)).start()
 
 
+    def left_dest(k):
+        return jnp.where(k < Z - 2, Z - 3 - k, Z - 2)
+
+    first = jnp.where(2 * z < Z, Z - 1 - left_dest(0), left_dest(0))
+    last = Z - 1 - z
+
+    def gate_up(k, parts, q):
+        lo, n = parts[0] * piece, len(parts) * piece
+        x = tok[pl.ds(2 * k, 2), lo:lo + n, pl.ds(pl.multiple_of(q * cw, cw), cw)].reshape(2 * n, cw)
+        return lax.dot_general(x, wbuf[q, 0:GU, :], CONTRACT, preferred_element_type=jnp.float32)
+
+    def prepare(slot, k, parts):
+        for h in parts:
+            tok_copy(2 * k + 1 - c, h, 0, partner).wait_recv()
+        pre[slot, 0:2 * len(parts) * piece] = gate_up(k, parts, f) + gate_up(k, parts, fx) + gate_up(k, parts, fy)
+
     if square:
         w_copy(0, fx, 0, fx).wait_recv()
         w_copy(1, fy, 1, fy).wait_recv()
+        if late:
+            @pl.when(end)
+            def _():
+                prepare(0, inner // 2, range(PARTS - HELD))
+                prepare(1, first, range(PARTS))
+
         w_copy(0, fd, 2, fx).wait_recv()
         w_copy(1, fd, 2, fy).wait_recv()
     else:
@@ -252,17 +274,20 @@
             w_copy(0, lax.rem(f + F - i, F), i, f).wait_recv()
     wt_all().wait_recv()
 
-    def hidden_rows(k, parts):
+    def hidden_rows(k, parts, slot=None):
         lo, n = parts[0] * piece, len(parts) * piece
-        for h in parts:
-            tok_copy(2 * k + 1 - c, h, 0, partner).wait_recv()
-        x = tok[pl.ds(2 * k, 2), lo:lo + n].reshape(2 * n, F * cw)
-        acc = jnp.zeros((2 * n, GU), jnp.float32)
-        for q in range(F):
-            acc = acc + lax.dot_general(
-                x[:, q * cw:(q + 1) * cw], wbuf[q, 0:GU, :], CONTRACT,
-                preferred_element_type=jnp.float32,
-            )
+        if slot is None or not square:
+            for h in parts:
+                tok_copy(2 * k + 1 - c, h, 0, partner).wait_recv()
+            x = tok[pl.ds(2 * k, 2), lo:lo + n].reshape(2 * n, F * cw)
+            acc = jnp.zeros((2 * n, GU), jnp.float32)
+            for q in range(F):
+                acc = acc + lax.dot_general(
+                    x[:, q * cw:(q + 1) * cw], wbuf[q, 0:GU, :], CONTRACT,
+                    preferred_element_type=jnp.float32,
+                )
+        else:
+            acc = pre[slot, 0:2 * n] + gate_up(k, parts, fd)
         g, u = acc[:, 0:H], acc[:, H:2 * H]
         sg, su = acc[:, 2 * H:2 * H + S], acc[:, 2 * H + S:GU]
         he = g / (1.0 + jnp.exp(-g)) * u
@@ -279,12 +304,6 @@
         hidden_rows(k, range(PARTS))
         return carry
 
-    def left_dest(k):
-        return jnp.where(k < Z - 2, Z - 3 - k, Z - 2)
-
-    first = jnp.where(2 * z < Z, Z - 1 - left_dest(0), left_dest(0))
-    last = Z - 1 - z
-
     def other_step(k, carry):
         @pl.when((k != first) & (k != z))
         def _():
@@ -302,10 +321,14 @@
     if late:
         @pl.when(end)
         def _():
-            hidden_rows(inner // 2, range(PARTS - HELD))
+            hidden_rows(inner // 2, range(PARTS - HELD), 0)
             send_hidden(0)
-
-        hidden_step(first, 0)
+            hidden_rows(first, range(PARTS), 1)
+
+        @pl.when(jnp.logical_not(end))
+        def _():
+            hidden_step(first, 0)
+
     else:
         lax.fori_loop(0, Z, hidden_step, 0)
 
@@ -759,6 +782,7 @@
             pltpu.VMEM((F * (Z + 1), M, cw), bf),
             pltpu.VMEM((2, F, H + S, cw), bf),
             pltpu.VMEM((2, M, HP), bf),
+            pltpu.VMEM((2, 2 * M, 2 * H + 2 * S), f32),
             dma((3,)),
             dma((T, PARTS)),
             dma((1,)),

time: 65.5 us -> 64.8 us (0.989)
  Pallas kernels: 64.7 us -> 64 us
    pallas_call x1, Pallas kernels: 62.7 us -> 61.9 us  [local(): pl.pallas_call(functools.partial(kernel, F, T, H, S, M), out_shape=[pltpu...]
where the time goes in v7:
time: 64.8 us; the launch traced here: 64.6 us
  Pallas kernels  64 us (99%)
    pallas_call x1, Pallas kernels, local(): pl.pallas_call(functools.partial(kernel, F, T, H, S, M), out_shape=[pltpu...  61.9 us
    pallas_call x1, Pallas kernels, local(): pl.pallas_call(functools.partial(place, H, S), out_shape=[jax.ShapeDtypeS...  2.08 us

profile of v7, /device:TPU:0, one launch (start us, length us, event | category | flops | bytes accessed | tf_op | source)
XLA Modules:
  0.0 64.6 jit_solution(3248384849919038035)
XLA Ops:
  0.6 61.9 %shard_map.153 = (bf16[4,960,512]{2,1,0:T(8,128)(2,1)S(1)}, bf16[4,128,512]{2,1,0:T(8,128)(2,1)S(1)}) custom-call(bf16[128,2048]{1,0:T(8,128)(2,1)} %tokens.1, f32[1,512]{1,0:T(1,128)} %bitcast.12, f32[256,512]{1,0:T(8,128)} %bitcast.9, f32[256,512]{1,0:T(8,128)} %bitcast.10, f32[256,512]{1,0:T(8,128)} %bitcast.11, f32[64,512]{1,0:T(8,128)} %sh_gate.1, ...), custom_call_target="tpu_custom_call" | custom-call | tf_op jit(solution)/shard_map/pallas_call | solution.py:769
  62.6 2.1 %shard_map.154 = (bf16[128,2048]{1,0:T(8,128)(2,1)}, bf16[256,2048]{1,0:T(8,128)(2,1)}, bf16[256,2048]{1,0:T(8,128)(2,1)}, bf16[256,2048]{1,0:T(8,128)(2,1)}, bf...) custom-call(bf16[4,960,512]{2,1,0:T(8,128)(2,1)S(1)} %get-tuple-element.16.wbuf, ...), custom_call_target="tpu_custom_call" | custom-call | tf_op jit(solution)/shard_map/pallas_call | solution.py:815

commit v8 on v7

--- a/solution.py
+++ b/solution.py
@@ -51,6 +51,7 @@
     late = Z >= 4
     HS = H + S
     strip = rows // SPLIT
+    slots = sin.shape[0] // F
     side_cols = cw // 2
     end = (z == 0) | (z == Z - 1)
     near = (z == 1) | (z == Z - 2)
@@ -170,7 +171,7 @@
         t = 2 * (inner // 2) + core
         return rdma(
             hid.at[t, part], hid2.at[sender, part],
-            z_send.at[1 + 2 * h + core], z_recv.at[1 + 2 * h + sender], (f, t),
+            z_send.at[1], z_recv.at[1 + 2 * h + sender], (f, t),
         )
 
     def send_hidden(h):
@@ -383,7 +384,7 @@
 
     def pass_piece(o, j, d, p, h):
         p = lax.rem(p, ring)
-        first_slot = j * (Z + 1)
+        first_slot = j * slots
         if late:
             from_left = (z > 0) & ((d > z) | ((d == z) & (z > 1)))
             from_right = (z < Z - 1) & ((d < z) | ((d == z) & (z < Z - 2)))
@@ -399,7 +400,7 @@
 
         @pl.when(from_right)
         def _():
-            slot = first_slot + jnp.where(d == z, Z, d)
+            slot = first_slot + (d if slots == Z else jnp.where(d == z, Z, d))
             sum_copy(0, h, slot, me).wait_recv()
             own[o, part] = own[o, part] + sin[slot, part].astype(jnp.float32)
 
@@ -413,7 +414,7 @@
 
         @pl.when(d < z)
         def _():
-            sum_copy(p, h, first_slot + jnp.where(d == z - 1, Z, d), left(me)).start()
+            sum_copy(p, h, first_slot + (d if slots == Z else jnp.where(d == z - 1, Z, d)), left(me)).start()
 
         @pl.when(d == z)
         def _():
@@ -688,9 +689,8 @@
         @pl.when(end)
         def _():
             end_weights().wait_send()
-            for h in range(2):
-                for core in range(2):
-                    end_hidden(h, core, c).wait_send()
+            block = hid.at[pl.ds(0, 2)]
+            rdma(block, hid2, z_send.at[1], z_recv.at[1], (f, inner)).wait_send()
 
         @pl.when(near)
         def _():
@@ -763,6 +763,7 @@
     Z = T // 2
     N, U = (Z - 1) * F, Z * F
     ring = min(U, RING)
+    slots = Z if Z == 4 else Z + 1
     HP = -(-(H + S) // 128) * 128
     bf, f32 = jnp.bfloat16, jnp.float32
     dma = pltpu.SemaphoreType.DMA
@@ -779,7 +780,7 @@
             pltpu.VMEM((ring, M, cw), bf),
             pltpu.VMEM((U, M, cw), bf),
             pltpu.VMEM((ring, M, cw), bf),
-            pltpu.VMEM((F * (Z + 1), M, cw), bf),
+            pltpu.VMEM((F * slots, M, cw), bf),
             pltpu.VMEM((2, F, H + S, cw), bf),
             pltpu.VMEM((2, M, HP), bf),
             pltpu.VMEM((2, 2 * M, 2 * H + 2 * S), f32),
@@ -792,11 +793,11 @@
             dma((ring if U > ring else 1,)),
             dma((U,)),
             dma((ring, SPLIT) if U > ring else (1, 1)),
-            dma((F * (Z + 1), SPLIT)),
+            dma((F * slots, SPLIT)),
             dma((1, F)),
             dma((2, F)),
             dma((2,)),
-            dma((5,)),
+            dma((2,)),
             dma((5,)),
             pltpu.VMEM((3 * H + 3 * S, cw), f32),
             pltpu.VMEM((M, D), bf),

time: 64.8 us -> 64.5 us (level)
  no operation moved by 1% of the time
where the time goes in v8:
time: 64.5 us; the launch traced here: 64.4 us
  Pallas kernels  63.7 us (99%)
    pallas_call x1, Pallas kernels, local(): pl.pallas_call(functools.partial(kernel, F, T, H, S, M), out_shape=[pltpu...  61.7 us
    pallas_call x1, Pallas kernels, local(): pl.pallas_call(functools.partial(place, H, S), out_shape=[jax.ShapeDtypeS...  2.08 us

profile of v8, /device:TPU:0, one launch (start us, length us, event | category | flops | bytes accessed | tf_op | source)
XLA Modules:
  0.0 64.4 jit_solution(16116105471880921169)
XLA Ops:
  0.6 61.7 %shard_map.153 = (bf16[4,960,512]{2,1,0:T(8,128)(2,1)S(1)}, bf16[4,128,512]{2,1,0:T(8,128)(2,1)S(1)}) custom-call(bf16[128,2048]{1,0:T(8,128)(2,1)} %tokens.1, f32[1,512]{1,0:T(1,128)} %bitcast.12, f32[256,512]{1,0:T(8,128)} %bitcast.9, f32[256,512]{1,0:T(8,128)} %bitcast.10, f32[256,512]{1,0:T(8,128)} %bitcast.11, f32[64,512]{1,0:T(8,128)} %sh_gate.1, ...), custom_call_target="tpu_custom_call" | custom-call | tf_op jit(solution)/shard_map/pallas_call | solution.py:770
  62.3 2.1 %shard_map.154 = (bf16[128,2048]{1,0:T(8,128)(2,1)}, bf16[256,2048]{1,0:T(8,128)(2,1)}, bf16[256,2048]{1,0:T(8,128)(2,1)}, bf16[256,2048]{1,0:T(8,128)(2,1)}, bf...) custom-call(bf16[4,960,512]{2,1,0:T(8,128)(2,1)S(1)} %get-tuple-element.16.wbuf, ...), custom_call_target="tpu_custom_call" | custom-call | tf_op jit(solution)/shard_map/pallas_call | solution.py:816
